TPU v7x, 32 devices: a whole 2x2x4 slice. The times are simulated.
32 devices in a mesh: sp: 16 (over z, y, core), tp: 2 (over x).
Axes of the slice: x: 2, y: 2, z: 4, core: 2. Of those that a mesh axis runs over, the one named last changes fastest.
Arguments:
- query_rows: bfloat16 [10240, 1536], P('sp', 'tp'), may hold values from -8 to 8
- key_rows: bfloat16 [10240, 1536], P('sp', 'tp'), may hold values from -8 to 8
- value_rows: bfloat16 [10240, 1536], P('sp', 'tp'), may hold values from -6 to 6
- query_gain: bfloat16 [64], replicated, may hold values from 0.25 to 4.2
- key_gain: bfloat16 [64], replicated, may hold values from 0.25 to 4.2
- position_bias: bfloat16 [24, 320], P('tp'), may hold values from -165 to 3
- output_grad: bfloat16 [10240, 1536], P('sp', 'tp'), may hold values from -24 to 24
Outputs:
- query_grad: bfloat16 [10240, 1536], P('sp', 'tp')
- key_grad: bfloat16 [10240, 1536], P('sp', 'tp')
- value_grad: bfloat16 [10240, 1536], P('sp', 'tp')
- bias_grad: float32 [24, 320], P('tp')
- query_gain_grad: float32 [64], replicated
- key_gain_grad: float32 [64], replicated
All inputs are finite; a program needn't handle non-finite values.
Results may differ from a plain program's by a relative error of at most 0.0055.
The roundings to bfloat16 on the way count: a program that leaves them out, or rounds other values in their place, can miss the bound.
Values may be sent and summed in bfloat16 or wider, within the bound.
A program may use at most 128 MiB of HBM per device.

v0:
```python
import functools

import jax
import jax.numpy as jnp
from jax import lax
from jax.experimental import pallas as pl
from jax.experimental.pallas import tpu as pltpu
from jax.sharding import PartitionSpec as P

SEG = 64
LEFT = 8
REACH = SEG * LEFT
RSPAN = 320
NORM_EPS = 1e-06
BLK = 2 * SEG
BAND = REACH + BLK
NEG = -1e30
F32 = jnp.float32
BF16 = jnp.bfloat16


def dot(a, b, dims):
    return lax.dot_general(a, b, (dims, ((), ())), preferred_element_type=F32)


def half_ones():
    row = lax.broadcasted_iota(jnp.int32, (BLK, BLK), 0) // 64
    col = lax.broadcasted_iota(jnp.int32, (BLK, BLK), 1) // 64
    return jnp.where(row == col, 1.0, 0.0).astype(BF16)


def head_mean(x, ones):
    high = x.astype(BF16)
    low = (x - high.astype(F32)).astype(BF16)
    return (dot(high, ones, ((1,), (0,))) + dot(low, ones, ((1,), (0,)))) * (1.0 / 64.0)


def normed(rows, ones):
    wide = rows.astype(F32)
    scale = lax.rsqrt(head_mean(wide * wide, ones) + NORM_EPS)
    return wide * scale, scale


def norm_grad(d_unit, gain, hat, scale, ones):
    scaled = d_unit * gain
    return scale * (scaled - hat * head_mean(scaled * hat, ones))


def stack_halves(x):
    lane = lax.broadcasted_iota(jnp.int32, x.shape, 1)
    zero = jnp.zeros_like(x)
    return jnp.concatenate([jnp.where(lane < 64, x, zero), jnp.where(lane < 64, zero, x)], axis=0)


def build_bias(table_row, bias_ref, head):
    wide = jnp.broadcast_to(table_row, (8, 512))
    sub = lax.broadcasted_iota(jnp.int32, (8, 512), 0)
    for bit in (1, 2, 4):
        wide = jnp.where((sub & bit) != 0, pltpu.roll(wide, bit, 1), wide)
    half = 8
    while half < BLK:
        wide = jnp.concatenate([wide, pltpu.roll(wide, half, 1)], axis=0)
        half *= 2
    lanes = slice(head * BLK, (head + 1) * BLK)
    row = lax.broadcasted_iota(jnp.int32, (BLK, BLK), 0)
    col = lax.broadcasted_iota(jnp.int32, (BLK, BLK), 1)
    far = jnp.broadcast_to(table_row[:, 0:1], (BLK, BLK))
    bias_ref[0:BLK, lanes] = jnp.where((row < SEG) & (col >= SEG), NEG, far)
    bias_ref[BLK : 2 * BLK, lanes] = far
    for j in range(3):
        tile = wide[:, ((4 - j) % 4) * BLK : ((4 - j) % 4) * BLK + BLK]
        if j == 2:
            tile = jnp.where((row >= SEG) & (col < SEG), NEG, tile)
        bias_ref[(2 + j) * BLK : (3 + j) * BLK, lanes] = tile


def fold_bias(acc_ref, head):
    lanes = slice(head * BLK, (head + 1) * BLK)
    tiles = [acc_ref[j * BLK : (j + 1) * BLK, lanes] for j in range(3)]
    wide = jnp.concatenate([tiles[0], jnp.zeros_like(tiles[0]), tiles[2], tiles[1]], axis=1)
    half = BLK // 2
    while half >= 8:
        wide = wide[:half] + pltpu.roll(wide[half:], 512 - half, 1)
        half //= 2
    for half in (4, 2, 1):
        wide = wide + pltpu.roll(pltpu.roll(wide, 512 - half, 1), 8 - half, 0)
    return wide[0:1]


def rounds_of(axis, size):
    rounds, stride = [], 1
    while stride < size:
        radix = 4 if size // stride % 4 == 0 else 2
        rounds.append((axis, stride, radix))
        stride *= radix
    return rounds


def peer(index, stride, radix, step):
    digit = (index // stride) % radix
    return index + stride * ((digit + step) % radix - digit)


def kernel(
    sp, tp, q_hbm, k_hbm, v_hbm, g_hbm, gains_ref, table_ref,
    qg_ref, kg_ref, vg_ref, out_ref,
    q_ref, k_ref, v_ref, g_ref,
    k_s, kt_s, v_s, bias_s, acc_s, s_s, dw_s, ds_s, w_s, qs_s, gs_s, hat_s, scale_s, dk_s, dv_s, clip_s, gq_s, gk_s,
    pk_s, pv_s, ck_s, cv_s, bk_s, bv_s, stat_s, got_s,
    prior_send, prior_recv, cross_send, cross_recv, stat_send, stat_recv, load_sem,
):
    tokens = q_ref.shape[0]
    blocks = tokens // BLK
    pairs = pk_s.shape[0]
    me = lax.axis_index("sp")
    me_tp = lax.axis_index("tp")
    right, left = lax.rem(me + 1, sp), lax.rem(me + sp - 1, sp)
    rounds = rounds_of("sp", sp) + rounds_of("tp", tp)
    peers = [
        [{axis: peer(me if axis == "sp" else me_tp, stride, radix, k)} for k in range(1, radix)]
        for axis, stride, radix in rounds
    ]
    first = me == 0

    def lanes_of(p):
        return pl.ds(pl.multiple_of(p * BLK, BLK), BLK)

    def loads(p):
        moves = ((k_hbm, k_ref), (q_hbm, q_ref), (v_hbm, v_ref), (g_hbm, g_ref))
        return [
            pltpu.make_async_copy(src.at[:, lanes_of(p)], dst.at[:, lanes_of(p)], load_sem.at[n, p])
            for n, (src, dst) in enumerate(moves)
        ]

    for p in range(pairs):
        for copy in loads(p):
            copy.start()

    barrier = pltpu.get_barrier_semaphore()
    greeted = [{"sp": right}, {"sp": left}] + [device for group in peers for device in group]
    for device in greeted:
        pl.semaphore_signal(barrier, inc=1, device_id=device, device_id_type=pl.DeviceIdType.MESH)
    pl.semaphore_wait(barrier, len(greeted))

    def remote(src, dst, send, recv, device):
        return pltpu.make_async_remote_copy(
            src_ref=src, dst_ref=dst, send_sem=send, recv_sem=recv,
            device_id=device, device_id_type=pl.DeviceIdType.MESH,
        )

    def prior_copies(p):
        rows = slice(tokens - REACH, tokens)
        return (
            remote(k_hbm.at[rows, lanes_of(p)], pk_s.at[p], prior_send.at[0, p], prior_recv.at[0, p], {"sp": right}),
            remote(v_hbm.at[rows, lanes_of(p)], pv_s.at[p], prior_send.at[1, p], prior_recv.at[1, p], {"sp": right}),
        )

    def cross_copies(p):
        return (
            remote(ck_s.at[p], bk_s.at[p], cross_send.at[0, p], cross_recv.at[0, p], {"sp": left}),
            remote(cv_s.at[p], bv_s.at[p], cross_send.at[1, p], cross_recv.at[1, p], {"sp": left}),
        )

    for p in range(pairs):
        for copy in prior_copies(p):
            copy.start()

    ones = half_ones()
    gain_q = gains_ref[0:1, :]
    gain_k = gains_ref[1:2, :]
    stat_s[0] = jnp.zeros(stat_s.shape[1:], F32)
    gq_s[...] = jnp.zeros_like(gq_s)
    gk_s[...] = jnp.zeros_like(gk_s)

    def key_tile(raw, b):
        unit = normed(raw, ones)[0] * gain_k
        k_s[b * BLK : (b + 1) * BLK, :] = unit.astype(BF16)
        kt_s[:, b * BLK : (b + 1) * BLK] = unit.T.astype(BF16)

    def finish(p):
        slot = lax.rem(p, 2)
        for copy in cross_copies(p):
            copy.wait_recv()
        total = jnp.zeros((1, BLK), F32)
        for b in range(blocks):
            rows = slice(b * BLK, (b + 1) * BLK)
            hat, scale = normed(k_ref[rows, lanes_of(p)], ones)
            ext = slice(REACH + b * BLK, REACH + (b + 1) * BLK)
            dk, dv = dk_s[slot, ext, :], dv_s[slot, ext, :]
            back = b * BLK - (tokens - REACH)
            if back >= 0:
                dk = dk + bk_s[p, back : back + BLK, :].astype(F32)
                dv = dv + bv_s[p, back : back + BLK, :].astype(F32)
            total = total + jnp.sum(dk * hat, axis=0, keepdims=True)
            kg_ref[rows, lanes_of(p)] = norm_grad(dk, gain_k, hat, scale, ones).astype(BF16)
            vg_ref[rows, lanes_of(p)] = dv.astype(BF16)
        gk_s[...] += total

    def pair(p, _):
        slot = lax.rem(p, 2)
        for head in range(2):
            build_bias(table_ref[pl.ds(p * 2 + head, 1), :], bias_s, head)
        dk_s[slot] = jnp.zeros(dk_s.shape[1:], F32)
        dv_s[slot] = jnp.zeros(dv_s.shape[1:], F32)
        acc_s[...] = jnp.zeros_like(acc_s)
        clip_s[...] = jnp.zeros_like(clip_s)
        for copy in loads(p):
            copy.wait()
        for b in range(blocks):
            rows = slice(b * BLK, (b + 1) * BLK)
            key_tile(k_ref[rows, lanes_of(p)], b + LEFT // 2)
            hat, scale = normed(q_ref[rows, lanes_of(p)], ones)
            hat_s[rows, :] = hat
            scale_s[rows, :] = scale
            qs_s[b] = stack_halves((hat * gain_q).astype(BF16) * jnp.asarray(0.125, BF16))
            gs_s[b] = stack_halves(g_ref[rows, lanes_of(p)])
        v_s[REACH:, :] = v_ref[:, lanes_of(p)]
        for copy in prior_copies(p):
            copy.wait_recv()
        for b in range(LEFT // 2):
            key_tile(pk_s[p, b * BLK : (b + 1) * BLK, :], b)
        v_s[:REACH, :] = pv_s[p]

        def tile(j):
            return slice(j * BLK, (j + 1) * BLK)

        def score(i, j, peaks):
            keys = tile(i + j)
            s = dot(k_s[keys, :], qs_s[i], ((1,), (1,))) + bias_s[tile(j), :]
            s_s[i % 2, tile(j), :] = s
            dw_s[i % 2, tile(j), :] = dot(v_s[keys, :], gs_s[i], ((1,), (1,)))
            top = jnp.max(s, axis=0, keepdims=True)
            peaks.append(top + penalty if j < LEFT // 2 - i else top)

        def product(i, j):
            keys = tile(i + j)
            dk_s[slot, keys, :] += dot(ds_s[i % 2, tile(j), :], qs_s[i], ((1,), (0,)))
            dv_s[slot, keys, :] += dot(w_s[i % 2, tile(j), :], gs_s[i], ((1,), (0,)))

        def query_side(i):
            rows = tile(i)
            dqt = dot(kt_s[:, i * BLK : i * BLK + BAND], ds_s[i % 2], ((1,), (0,)))
            dqt = jnp.concatenate([dqt[:64, :BLK], dqt[64:, BLK:]], axis=0)
            dq = dqt.T * 0.125
            hat = hat_s[rows, :]
            gq_s[...] += jnp.sum(dq * hat, axis=0, keepdims=True)
            qg_ref[rows, lanes_of(p)] = norm_grad(dq, gain_q, hat, scale_s[rows, :], ones).astype(BF16)

        penalty = jnp.where(first, NEG, 0.0)
        peaks = {}
        for step in range(blocks + 2):
            ahead, here, behind = step, step - 1, step - 2
            peaks[ahead] = []
            if 0 <= here < blocks:
                peak = functools.reduce(jnp.maximum, peaks[here])
                total = jnp.zeros((1, 2 * BLK), F32)
                delta = jnp.zeros((1, 2 * BLK), F32)
                clipped = jnp.zeros((1, 2 * BLK), F32)
            for j in range(5):
                if ahead < blocks:
                    score(ahead, j, peaks[ahead])
                if 0 <= here < blocks:
                    e = jnp.exp(s_s[here % 2, tile(j), :] - (peak - penalty if j < LEFT // 2 - here else peak))
                    s_s[here % 2, tile(j), :] = e
                    total = total + jnp.sum(e, axis=0, keepdims=True)
                    delta = delta + jnp.sum(e * dw_s[here % 2, tile(j), :], axis=0, keepdims=True)
            if 0 <= here < blocks:
                inverse = 1.0 / total
                delta = delta * inverse
            if behind >= 0:
                query_side(behind)
            for j in range(5):
                if behind >= 0:
                    product(behind, j)
                if 0 <= here < blocks:
                    w = s_s[here % 2, tile(j), :] * inverse
                    ds = w * (dw_s[here % 2, tile(j), :] - delta)
                    if j < 2:
                        clipped = clipped + jnp.sum(ds, axis=0, keepdims=True)
                    else:
                        acc_s[tile(j - 2), :] += ds
                    ds_s[here % 2, tile(j), :] = ds.astype(BF16)
                    w_s[here % 2, tile(j), :] = w.astype(BF16)
            if 0 <= here < blocks:
                clip_s[...] += clipped
        ck_s[p] = dk_s[slot, :REACH, :].astype(BF16)
        cv_s[p] = dv_s[slot, :REACH, :].astype(BF16)
        lane = lax.broadcasted_iota(jnp.int32, (1, 512), 1)
        for head in range(2):
            far = jnp.sum(clip_s[:, head * BLK : (head + 1) * BLK], axis=1, keepdims=True)
            stat_s[0, pl.ds(p * 2 + head, 1), :] = fold_bias(acc_s, head) + jnp.where(lane == 0, far, 0.0)
        for copy in cross_copies(p):
            copy.start()

        @pl.when(p > 0)
        def _():
            finish(p - 1)

        return 0

    lax.fori_loop(0, pairs, pair, 0)
    finish(pairs - 1)
    rows = stat_s.shape[1]
    stat_s[0, rows - 8 : rows - 7, 0:BLK] = gq_s[...]
    stat_s[0, rows - 8 : rows - 7, BLK : 2 * BLK] = gk_s[...]
    summed = len(rounds_of("sp", sp))
    for r, group in enumerate(peers):
        part = slice(0, rows) if r < summed else slice(rows - 8, rows)
        copies = [
            remote(stat_s.at[r, part], got_s.at[r, k, part], stat_send.at[r, k], stat_recv.at[r, k], device)
            for k, device in enumerate(group)
        ]
        for copy in copies:
            copy.start()
        for copy in copies:
            copy.wait()
        if len(group) == 3:
            stat_s[r + 1, part] = (stat_s[r, part] + got_s[r, 1, part]) + (got_s[r, 0, part] + got_s[r, 2, part])
        else:
            stat_s[r + 1, part] = stat_s[r, part] + got_s[r, 0, part]
    out_ref[: rows - 8, :] = stat_s[summed, : rows - 8]
    out_ref[rows - 8 :, :] = stat_s[len(peers), rows - 8 :]
    for p in range(pairs):
        for copy in prior_copies(p) + cross_copies(p):
            copy.wait_send()


def body(query_rows, key_rows, value_rows, query_gain, key_gain, position_bias, output_grad):
    heads = position_bias.shape[0]
    pairs = heads // 2
    tokens = query_rows.shape[0]
    sp, tp = lax.axis_size("sp"), lax.axis_size("tp")
    rounds = len(rounds_of("sp", sp) + rounds_of("tp", tp))
    table = position_bias.astype(F32)
    last = jnp.broadcast_to(table[:, -1:], (heads, 129))
    table = jnp.concatenate([last, jnp.full((heads, 64), NEG, F32), table[:, :-1]], axis=1)
    gains = jnp.stack([jnp.tile(query_gain.astype(F32), 2), jnp.tile(key_gain.astype(F32), 2)])
    ext = tokens + REACH
    rows = (heads + 7) // 8 * 8 + 8
    vmem = pl.BlockSpec(memory_space=pltpu.VMEM)
    grads = jax.ShapeDtypeStruct((tokens, heads * 64), BF16)
    sems = pltpu.SemaphoreType.DMA
    query_grad, key_grad, value_grad, stats = pl.pallas_call(
        functools.partial(kernel, sp, tp),
        in_specs=[pl.BlockSpec(memory_space=pltpu.HBM)] * 4 + [vmem] * 2,
        out_specs=[vmem] * 4,
        out_shape=[grads, grads, grads, jax.ShapeDtypeStruct((rows, 512), F32)],
        scratch_shapes=[pltpu.VMEM((tokens, heads * 64), BF16)] * 4
        + [
            pltpu.VMEM((ext, BLK), BF16), pltpu.VMEM((BLK, ext), BF16), pltpu.VMEM((ext, BLK), BF16),
            pltpu.VMEM((BAND, 2 * BLK), F32), pltpu.VMEM((3 * BLK, 2 * BLK), F32),
            pltpu.VMEM((2, BAND, 2 * BLK), F32), pltpu.VMEM((2, BAND, 2 * BLK), F32),
            pltpu.VMEM((2, BAND, 2 * BLK), BF16), pltpu.VMEM((2, BAND, 2 * BLK), BF16),
            pltpu.VMEM((tokens // BLK, 2 * BLK, BLK), BF16), pltpu.VMEM((tokens // BLK, 2 * BLK, BLK), BF16),
            pltpu.VMEM((tokens, BLK), F32), pltpu.VMEM((tokens, BLK), F32),
            pltpu.VMEM((2, ext, BLK), F32), pltpu.VMEM((2, ext, BLK), F32),
            pltpu.VMEM((1, 2 * BLK), F32), pltpu.VMEM((1, BLK), F32), pltpu.VMEM((1, BLK), F32),
        ]
        + [pltpu.VMEM((pairs, REACH, BLK), BF16)] * 6
        + [
            pltpu.VMEM((rounds + 1, rows, 512), F32), pltpu.VMEM((rounds, 3, rows, 512), F32),
            sems((2, pairs)), sems((2, pairs)), sems((2, pairs)), sems((2, pairs)),
            sems((rounds, 3)), sems((rounds, 3)), sems((4, pairs)),
        ],
        compiler_params=pltpu.CompilerParams(collective_id=0, has_side_effects=True, vmem_limit_bytes=48 << 20),
        name="attend",
    )(query_rows, key_rows, value_rows, output_grad, gains, table)
    fold = stats[:heads]
    bias_grad = jnp.concatenate([fold[:, 193:], jnp.sum(fold[:, :129], axis=1, keepdims=True)], axis=1)
    gain_row = stats[rows - 8]
    query_gain_grad = gain_row[:64] + gain_row[64:128]
    key_gain_grad = gain_row[128:192] + gain_row[192:256]
    return (query_grad, key_grad, value_grad, bias_grad, query_gain_grad, key_gain_grad)


def solution(mesh):
    placed = (P("sp", "tp"), P("sp", "tp"), P("sp", "tp"), P(), P(), P("tp", None), P("sp", "tp"))
    return jax.shard_map(
        body,
        mesh=mesh,
        in_specs=placed,
        out_specs=(P("sp", "tp"), P("sp", "tp"), P("sp", "tp"), P("tp", None), P(), P()),
        check_vma=False,
    )
```

profile of v0, /device:TPU:0, one launch (start us, length us, event | category | flops | bytes accessed | tf_op | source)
XLA Modules:
  0.0 74.0 jit_solution(14890223110260275351)
XLA Ops:
  0.6 0.7 convert_element_type.11
  1.3 0.0 copy-start.3
  1.3 0.2 slice_reduce_fusion.1
  1.5 0.1 broadcast_in_dim.14
  1.6 0.4 copy-done.3
  2.1 0.1 pad.3.clone
  2.1 0.0 copy-start.4
  2.1 0.1 pad_maximum_fusion.table_ref
  2.2 0.6 copy-done.4
  2.8 0.0 copy-start.5
  2.8 0.1 stack_tile.6
  2.9 0.6 copy-done.5
  3.5 0.1 stack_tile.7
  3.5 0.0 copy-start
  3.6 1.2 %copy-done = bf16[640,768]{1,0:T(8,128)(2,1)S(1)} copy-done((bf16[640,768]{1,0:T(8,128)(2,1)S(1)}, bf16[640,768]{1,0:T(8,128)(2,1)}, u32[]{:S(2)}) %copy-start) | copy-done | bytes 983064
  4.8 0.0 copy-start.1
  4.8 1.2 %copy-done.1 = bf16[640,768]{1,0:T(8,128)(2,1)S(1)} copy-done((bf16[640,768]{1,0:T(8,128)(2,1)S(1)}, bf16[640,768]{1,0:T(8,128)(2,1)}, u32[]{:S(2)}) %copy-start.1) | copy-done | bytes 983064
  6.0 0.0 copy-start.2
  6.0 1.2 %copy-done.2 = bf16[640,768]{1,0:T(8,128)(2,1)S(1)} copy-done((bf16[640,768]{1,0:T(8,128)(2,1)S(1)}, bf16[640,768]{1,0:T(8,128)(2,1)}, u32[]{:S(2)}) %copy-start.2) | copy-done | bytes 983064
  7.2 62.5 %attend.1 = (bf16[640,768]{1,0:T(8,128)(2,1)S(1)}, bf16[640,768]{1,0:T(8,128)(2,1)S(1)}, bf16[640,768]{1,0:T(8,128)(2,1)S(1)}, f32[24,512]{1,0:T(8,128)S(1)}) custom-call(bf16[640,768]{1,0:T(8,128)(2,1)S(1)} %copy-done, bf16[640,768]{1,0:T(8,128)(2,1)S(1)} %copy-done.1, bf16[640,768]{1,0:T(8,128)(2,1)S(1)} %copy-done.2, bf16[640,768]{1,0:T(8,128)(2,1)} %g_hbm.1, ...), custom_call_target="tpu_custom_call" | custom-call | tf_op jit(solution)/shard_map/attend/pallas_call | solution.py:343
  69.6 0.1 slice.38
  69.7 0.1 slice_reduce_fusion
  69.8 0.1 copy.14
  69.9 0.7 pad_maximum_fusion.1
  70.6 0.6 add_bitcast_fusion
  71.2 0.9 %copy.18 = bf16[640,768]{1,0:T(8,128)(2,1)} copy(bf16[640,768]{1,0:T(8,128)(2,1)S(1)} %get-tuple-element.22) | data formatting | bytes 1966080
  72.1 0.9 %copy.19 = bf16[640,768]{1,0:T(8,128)(2,1)} copy(bf16[640,768]{1,0:T(8,128)(2,1)S(1)} %get-tuple-element.23) | data formatting | bytes 1966080
  73.1 0.9 %copy.20 = bf16[640,768]{1,0:T(8,128)(2,1)} copy(bf16[640,768]{1,0:T(8,128)(2,1)S(1)} %get-tuple-element.24) | data formatting | bytes 1966080
  (5 shorter events, 0.0 us)
Async XLA Ops:
  1.3 0.7 copy-start.3
  2.1 0.7 copy-start.4
  2.8 0.7 copy-start.5
  3.5 1.2 %copy-start = (bf16[640,768]{1,0:T(8,128)(2,1)S(1)}, bf16[640,768]{1,0:T(8,128)(2,1)}, u32[]{:S(2)}) copy-start(bf16[640,768]{1,0:T(8,128)(2,1)} %q_hbm.1) | copy-start | bytes 2949124
  4.8 1.2 %copy-start.1 = (bf16[640,768]{1,0:T(8,128)(2,1)S(1)}, bf16[640,768]{1,0:T(8,128)(2,1)}, u32[]{:S(2)}) copy-start(bf16[640,768]{1,0:T(8,128)(2,1)} %k_hbm.1) | copy-start | bytes 2949124
  6.0 1.2 %copy-start.2 = (bf16[640,768]{1,0:T(8,128)(2,1)S(1)}, bf16[640,768]{1,0:T(8,128)(2,1)}, u32[]{:S(2)}) copy-start(bf16[640,768]{1,0:T(8,128)(2,1)} %v_hbm.1) | copy-start | bytes 2949124
where the time goes:
time: 74.4 us; the launch traced here: 74 us
  Pallas kernels  62.5 us (84%)
  local copies, waits for them, and re-layouts  8.71 us (12%)
  other arithmetic  2.19 us (3%)
    pallas_call x1, Pallas kernels, body(): pl.pallas_call(functools.partial(kernel, sp, tp), in_specs=[pl.BlockSpec(...  62.5 us
    unnamed x15, local copies, waits for them, and re-layouts  8.03 us

commit v1 on v0

--- a/solution.py
+++ b/solution.py
@@ -87,11 +87,11 @@
     return wide[0:1]
 
 
-def rounds_of(axis, size):
+def rounds_of(size):
     rounds, stride = [], 1
     while stride < size:
         radix = 4 if size // stride % 4 == 0 else 2
-        rounds.append((axis, stride, radix))
+        rounds.append((stride, radix))
         stride *= radix
     return rounds
 
@@ -101,13 +101,20 @@
     return index + stride * ((digit + step) % radix - digit)
 
 
+def ring_sum(parts):
+    if len(parts) == 4:
+        return (parts[0] + parts[2]) + (parts[1] + parts[3])
+    return parts[0] + parts[1] if len(parts) == 2 else parts[0]
+
+
 def kernel(
-    sp, tp, q_hbm, k_hbm, v_hbm, g_hbm, gains_ref, table_ref,
+    sp, tp, q_hbm, k_hbm, v_hbm, g_hbm, qgain_hbm, kgain_hbm, table_hbm,
     qg_ref, kg_ref, vg_ref, out_ref,
     q_ref, k_ref, v_ref, g_ref,
     k_s, kt_s, v_s, bias_s, acc_s, s_s, dw_s, ds_s, w_s, qs_s, gs_s, hat_s, scale_s, dk_s, dv_s, clip_s, gq_s, gk_s,
-    pk_s, pv_s, ck_s, cv_s, bk_s, bv_s, stat_s, got_s,
-    prior_send, prior_recv, cross_send, cross_recv, stat_send, stat_recv, load_sem,
+    pk_s, pv_s, ck_s, cv_s, bk_s, bv_s, bsum_s, bgot_s, gsum_s, ggot_s, gfirst_s,
+    qgain_s, kgain_s, raw_s, wide_s, table_s, gains_s,
+    prior_send, prior_recv, cross_send, cross_recv, bias_send, bias_recv, gain_send, gain_recv, load_sem, small_sem,
 ):
     tokens = q_ref.shape[0]
     blocks = tokens // BLK
@@ -115,12 +122,12 @@
     me = lax.axis_index("sp")
     me_tp = lax.axis_index("tp")
     right, left = lax.rem(me + 1, sp), lax.rem(me + sp - 1, sp)
-    rounds = rounds_of("sp", sp) + rounds_of("tp", tp)
-    peers = [
-        [{axis: peer(me if axis == "sp" else me_tp, stride, radix, k)} for k in range(1, radix)]
-        for axis, stride, radix in rounds
-    ]
-    first = me == 0
+    rounds = rounds_of(sp)
+    count = len(rounds)
+    peers = [[{"sp": peer(me, stride, radix, k)} for k in range(1, radix)] for stride, radix in rounds]
+    combos = [(k, t) for k in range(rounds[0][1]) for t in range(tp) if k or t]
+    nearby = [{"sp": peer(me, 1, rounds[0][1], k), "tp": lax.rem(me_tp + t, tp)} for k, t in combos]
+    first, last = me == 0, me == sp - 1
 
     def lanes_of(p):
         return pl.ds(pl.multiple_of(p * BLK, BLK), BLK)
@@ -132,12 +139,18 @@
             for n, (src, dst) in enumerate(moves)
         ]
 
+    smalls = [
+        pltpu.make_async_copy(src, dst, small_sem.at[n])
+        for n, (src, dst) in enumerate(((qgain_hbm, qgain_s), (kgain_hbm, kgain_s), (table_hbm, raw_s)))
+    ]
+    for copy in smalls:
+        copy.start()
     for p in range(pairs):
         for copy in loads(p):
             copy.start()
 
     barrier = pltpu.get_barrier_semaphore()
-    greeted = [{"sp": right}, {"sp": left}] + [device for group in peers for device in group]
+    greeted = [{"sp": right}, {"sp": left}] + nearby + [device for group in peers for device in group]
     for device in greeted:
         pl.semaphore_signal(barrier, inc=1, device_id=device, device_id_type=pl.DeviceIdType.MESH)
     pl.semaphore_wait(barrier, len(greeted))
@@ -161,14 +174,82 @@
             remote(cv_s.at[p], bv_s.at[p], cross_send.at[1, p], cross_recv.at[1, p], {"sp": left}),
         )
 
-    for p in range(pairs):
-        for copy in prior_copies(p):
+    @pl.when(jnp.logical_not(last))
+    def _():
+        for p in range(pairs):
+            for copy in prior_copies(p):
+                copy.start()
+
+    @pl.when(first)
+    def _():
+        pk_s[...] = jnp.zeros_like(pk_s)
+        pv_s[...] = jnp.zeros_like(pv_s)
+
+    @pl.when(last)
+    def _():
+        bk_s[...] = jnp.zeros_like(bk_s)
+        bv_s[...] = jnp.zeros_like(bv_s)
+
+    def bias_copies(r, p):
+        return [
+            remote(bsum_s.at[r, p], bgot_s.at[r, p, k], bias_send.at[r, k, p], bias_recv.at[r, k, p], device)
+            for k, device in enumerate(peers[r])
+        ]
+
+    def bias_start(r, p):
+        for copy in bias_copies(r, p):
             copy.start()
 
+    def bias_add(r, p):
+        for copy in bias_copies(r, p):
+            copy.wait_recv()
+        bsum_s[r + 1, p] = ring_sum([bsum_s[r, p]] + [bgot_s[r, p, k] for k in range(len(peers[r]))])
+
+    def bias_step(r, p):
+        bias_add(r - 1, p)
+        if r < count:
+            bias_start(r, p)
+
+    def gain_copies(r):
+        if r == 0:
+            return [
+                remote(gsum_s.at[0], gfirst_s.at[n], gain_send.at[0, n], gain_recv.at[0, n], device)
+                for n, device in enumerate(nearby)
+            ]
+        return [
+            remote(gsum_s.at[r], ggot_s.at[r, k], gain_send.at[r, k], gain_recv.at[r, k], device)
+            for k, device in enumerate(peers[r])
+        ]
+
+    def gain_start(r):
+        for copy in gain_copies(r):
+            copy.start()
+
+    def gain_add(r):
+        for copy in gain_copies(r):
+            copy.wait_recv()
+        if r == 0:
+            parts = {combo: gfirst_s[n] for n, combo in enumerate(combos)}
+            parts[0, 0] = gsum_s[0]
+            gsum_s[1] = ring_sum([ring_sum([parts[k, t] for t in range(tp)]) for k in range(rounds[0][1])])
+        else:
+            gsum_s[r + 1] = ring_sum([gsum_s[r]] + [ggot_s[r, k] for k in range(len(peers[r]))])
+
     ones = half_ones()
-    gain_q = gains_ref[0:1, :]
-    gain_k = gains_ref[1:2, :]
-    stat_s[0] = jnp.zeros(stat_s.shape[1:], F32)
+    for copy in smalls:
+        copy.wait()
+    for half in range(2):
+        gains_s[0:1, half * 64 : half * 64 + 64] = qgain_s[...].astype(F32)
+        gains_s[1:2, half * 64 : half * 64 + 64] = kgain_s[...].astype(F32)
+    gain_q = gains_s[0:1, :]
+    gain_k = gains_s[1:2, :]
+    heads, span = raw_s.shape
+    wide_s[...] = jnp.zeros_like(wide_s)
+    wide_s[0:heads, 0:span] = raw_s[...].astype(F32)
+    wide = wide_s[...]
+    place = lax.broadcasted_iota(jnp.int32, wide.shape, 1)
+    moved = pltpu.roll(wide, 193, 1)
+    table_s[...] = jnp.where(place <= 128, wide[:, span - 1 : span], jnp.where(place < 193, NEG, moved))
     gq_s[...] = jnp.zeros_like(gq_s)
     gk_s[...] = jnp.zeros_like(gk_s)
 
@@ -179,8 +260,11 @@
 
     def finish(p):
         slot = lax.rem(p, 2)
-        for copy in cross_copies(p):
-            copy.wait_recv()
+        @pl.when(jnp.logical_not(last))
+        def _():
+            for copy in cross_copies(p):
+                copy.wait_recv()
+
         total = jnp.zeros((1, BLK), F32)
         for b in range(blocks):
             rows = slice(b * BLK, (b + 1) * BLK)
@@ -199,7 +283,7 @@
     def pair(p, _):
         slot = lax.rem(p, 2)
         for head in range(2):
-            build_bias(table_ref[pl.ds(p * 2 + head, 1), :], bias_s, head)
+            build_bias(table_s[pl.ds(p * 2 + head, 1), :], bias_s, head)
         dk_s[slot] = jnp.zeros(dk_s.shape[1:], F32)
         dv_s[slot] = jnp.zeros(dv_s.shape[1:], F32)
         acc_s[...] = jnp.zeros_like(acc_s)
@@ -215,8 +299,11 @@
             qs_s[b] = stack_halves((hat * gain_q).astype(BF16) * jnp.asarray(0.125, BF16))
             gs_s[b] = stack_halves(g_ref[rows, lanes_of(p)])
         v_s[REACH:, :] = v_ref[:, lanes_of(p)]
-        for copy in prior_copies(p):
-            copy.wait_recv()
+        @pl.when(jnp.logical_not(first))
+        def _():
+            for copy in prior_copies(p):
+                copy.wait_recv()
+
         for b in range(LEFT // 2):
             key_tile(pk_s[p, b * BLK : (b + 1) * BLK, :], b)
         v_s[:REACH, :] = pv_s[p]
@@ -285,12 +372,24 @@
                 clip_s[...] += clipped
         ck_s[p] = dk_s[slot, :REACH, :].astype(BF16)
         cv_s[p] = dv_s[slot, :REACH, :].astype(BF16)
+        @pl.when(jnp.logical_not(first))
+        def _():
+            for copy in cross_copies(p):
+                copy.start()
+
         lane = lax.broadcasted_iota(jnp.int32, (1, 512), 1)
+        rows = []
         for head in range(2):
             far = jnp.sum(clip_s[:, head * BLK : (head + 1) * BLK], axis=1, keepdims=True)
-            stat_s[0, pl.ds(p * 2 + head, 1), :] = fold_bias(acc_s, head) + jnp.where(lane == 0, far, 0.0)
-        for copy in cross_copies(p):
-            copy.start()
+            row = fold_bias(acc_s, head) + jnp.where(lane == 0, far, 0.0)
+            rows += [row[:, b * BLK : (b + 1) * BLK] for b in range(4)]
+        bsum_s[0, p] = jnp.concatenate(rows, axis=0)
+        bias_start(0, p)
+        for r in range(1, count + 1):
+
+            @pl.when(p >= r)
+            def _():
+                bias_step(r, p - r)
 
         @pl.when(p > 0)
         def _():
@@ -300,29 +399,69 @@
 
     lax.fori_loop(0, pairs, pair, 0)
     finish(pairs - 1)
-    rows = stat_s.shape[1]
-    stat_s[0, rows - 8 : rows - 7, 0:BLK] = gq_s[...]
-    stat_s[0, rows - 8 : rows - 7, BLK : 2 * BLK] = gk_s[...]
-    summed = len(rounds_of("sp", sp))
-    for r, group in enumerate(peers):
-        part = slice(0, rows) if r < summed else slice(rows - 8, rows)
-        copies = [
-            remote(stat_s.at[r, part], got_s.at[r, k, part], stat_send.at[r, k], stat_recv.at[r, k], device)
-            for k, device in enumerate(group)
-        ]
-        for copy in copies:
-            copy.start()
-        for copy in copies:
-            copy.wait()
-        if len(group) == 3:
-            stat_s[r + 1, part] = (stat_s[r, part] + got_s[r, 1, part]) + (got_s[r, 0, part] + got_s[r, 2, part])
-        else:
-            stat_s[r + 1, part] = stat_s[r, part] + got_s[r, 0, part]
-    out_ref[: rows - 8, :] = stat_s[summed, : rows - 8]
-    out_ref[rows - 8 :, :] = stat_s[len(peers), rows - 8 :]
+    gsum_s[0] = jnp.zeros(gsum_s.shape[1:], F32)
+    gsum_s[0, 0:1, :] = gq_s[...]
+    gsum_s[0, 1:2, :] = gk_s[...]
+    gain_start(0)
+    for t in range(count):
+        for r in range(1, count + 1):
+            if 0 <= pairs + t - r < pairs:
+                bias_step(r, pairs + t - r)
+        gain_add(t)
+        if t + 1 < count:
+            gain_start(t + 1)
     for p in range(pairs):
-        for copy in prior_copies(p) + cross_copies(p):
+        out_ref[p] = bsum_s[count, p]
+    out_ref[pairs] = gsum_s[count]
+
+    @pl.when(jnp.logical_not(last))
+    def _():
+        for p in range(pairs):
+            for copy in prior_copies(p):
+                copy.wait_send()
+
+    @pl.when(jnp.logical_not(first))
+    def _():
+        for p in range(pairs):
+            for copy in cross_copies(p):
+                copy.wait_send()
+
+    for r in range(count):
+        for p in range(pairs):
+            for copy in bias_copies(r, p):
+                copy.wait_send()
+        for copy in gain_copies(r):
             copy.wait_send()
+
+
+def drain(
+    qg_ref, kg_ref, vg_ref, stat_ref, qg_hbm, kg_hbm, vg_hbm, bias_hbm, gq_hbm, gk_hbm,
+    wide_s, bias_s, gq_s, gk_s, sem,
+):
+    moves = [(qg_ref, qg_hbm), (kg_ref, kg_hbm), (vg_ref, vg_hbm), (gq_s, gq_hbm), (gk_s, gk_hbm), (bias_s, bias_hbm)]
+    copies = [pltpu.make_async_copy(src, dst, sem.at[n]) for n, (src, dst) in enumerate(moves)]
+    for copy in copies[:3]:
+        copy.start()
+    heads, span = bias_s.shape
+    pairs = heads // 2
+    for row, ref in enumerate((gq_s, gk_s)):
+        both = stat_ref[pairs, row : row + 1, :]
+        ref[...] = (both + pltpu.roll(both, 64, 1))[:, :64].reshape(64)
+    copies[3].start()
+    copies[4].start()
+    wide_s[...] = jnp.zeros_like(wide_s)
+    for head in range(heads):
+        for b in range(4):
+            row = head % 2 * 4 + b
+            wide_s[head : head + 1, b * BLK : (b + 1) * BLK] = stat_ref[head // 2, row : row + 1, :]
+    wide = wide_s[...]
+    lane = lax.broadcasted_iota(jnp.int32, wide.shape, 1)
+    far = jnp.sum(jnp.where(lane <= 128, wide, 0.0), axis=1, keepdims=True)
+    folded = jnp.where(lane == span - 1, far, pltpu.roll(wide, 319, 1))
+    bias_s[...] = folded[:heads, :span]
+    copies[5].start()
+    for copy in copies:
+        copy.wait()
 
 
 def body(query_rows, key_rows, value_rows, query_gain, key_gain, position_bias, output_grad):
@@ -330,21 +469,23 @@
     pairs = heads // 2
     tokens = query_rows.shape[0]
     sp, tp = lax.axis_size("sp"), lax.axis_size("tp")
-    rounds = len(rounds_of("sp", sp) + rounds_of("tp", tp))
-    table = position_bias.astype(F32)
-    last = jnp.broadcast_to(table[:, -1:], (heads, 129))
-    table = jnp.concatenate([last, jnp.full((heads, 64), NEG, F32), table[:, :-1]], axis=1)
-    gains = jnp.stack([jnp.tile(query_gain.astype(F32), 2), jnp.tile(key_gain.astype(F32), 2)])
+    count = len(rounds_of(sp))
+    group = 4 * tp
     ext = tokens + REACH
-    rows = (heads + 7) // 8 * 8 + 8
-    vmem = pl.BlockSpec(memory_space=pltpu.VMEM)
-    grads = jax.ShapeDtypeStruct((tokens, heads * 64), BF16)
+    padded = (heads + 7) // 8 * 8
+    vmem, hbm = pl.BlockSpec(memory_space=pltpu.VMEM), pl.BlockSpec(memory_space=pltpu.HBM)
+    shape = jax.ShapeDtypeStruct
+    grads = shape((tokens, heads * 64), BF16)
     sems = pltpu.SemaphoreType.DMA
-    query_grad, key_grad, value_grad, stats = pl.pallas_call(
+    operands = (
+        query_rows, key_rows, value_rows, output_grad,
+        query_gain.reshape(1, 64), key_gain.reshape(1, 64), position_bias,
+    )
+    results = pl.pallas_call(
         functools.partial(kernel, sp, tp),
-        in_specs=[pl.BlockSpec(memory_space=pltpu.HBM)] * 4 + [vmem] * 2,
+        in_specs=[hbm] * 7,
         out_specs=[vmem] * 4,
-        out_shape=[grads, grads, grads, jax.ShapeDtypeStruct((rows, 512), F32)],
+        out_shape=[grads, grads, grads, shape((pairs + 1, 8, BLK), F32)],
         scratch_shapes=[pltpu.VMEM((tokens, heads * 64), BF16)] * 4
         + [
             pltpu.VMEM((ext, BLK), BF16), pltpu.VMEM((BLK, ext), BF16), pltpu.VMEM((ext, BLK), BF16),
@@ -358,19 +499,29 @@
         ]
         + [pltpu.VMEM((pairs, REACH, BLK), BF16)] * 6
         + [
-            pltpu.VMEM((rounds + 1, rows, 512), F32), pltpu.VMEM((rounds, 3, rows, 512), F32),
+            pltpu.VMEM((count + 1, pairs, 8, BLK), F32), pltpu.VMEM((count, pairs, 3, 8, BLK), F32),
+            pltpu.VMEM((count + 1, 8, BLK), F32), pltpu.VMEM((count, 3, 8, BLK), F32), pltpu.VMEM((group, 8, BLK), F32),
+            pltpu.VMEM((1, 64), BF16), pltpu.VMEM((1, 64), BF16), pltpu.VMEM(position_bias.shape, BF16),
+            pltpu.VMEM((padded, 512), F32), pltpu.VMEM((padded, 512), F32), pltpu.VMEM((8, BLK), F32),
             sems((2, pairs)), sems((2, pairs)), sems((2, pairs)), sems((2, pairs)),
-            sems((rounds, 3)), sems((rounds, 3)), sems((4, pairs)),
+            sems((count, 3, pairs)), sems((count, 3, pairs)), sems((count, group)), sems((count, group)),
+            sems((4, pairs)), sems((3,)),
         ],
         compiler_params=pltpu.CompilerParams(collective_id=0, has_side_effects=True, vmem_limit_bytes=48 << 20),
         name="attend",
-    )(query_rows, key_rows, value_rows, output_grad, gains, table)
-    fold = stats[:heads]
-    bias_grad = jnp.concatenate([fold[:, 193:], jnp.sum(fold[:, :129], axis=1, keepdims=True)], axis=1)
-    gain_row = stats[rows - 8]
-    query_gain_grad = gain_row[:64] + gain_row[64:128]
-    key_gain_grad = gain_row[128:192] + gain_row[192:256]
-    return (query_grad, key_grad, value_grad, bias_grad, query_gain_grad, key_gain_grad)
+    )(*[pltpu.with_memory_space_constraint(x, pltpu.HBM) for x in operands])
+    return pl.pallas_call(
+        drain,
+        in_specs=[vmem] * 4,
+        out_specs=[hbm] * 6,
+        out_shape=[grads, grads, grads, shape(position_bias.shape, F32), shape((64,), F32), shape((64,), F32)],
+        scratch_shapes=[
+            pltpu.VMEM((padded, 512), F32), pltpu.VMEM(position_bias.shape, F32),
+            pltpu.VMEM((64,), F32), pltpu.VMEM((64,), F32), sems((6,)),
+        ],
+        compiler_params=pltpu.CompilerParams(vmem_limit_bytes=2 << 20),
+        name="drain",
+    )(*results)
 
 
 def solution(mesh):

time: 74.4 us -> 67.8 us (0.911)
  local copies, waits for them, and re-layouts: 8.71 us -> 0 us
  Pallas kernels: 62.5 us -> 67 us
  other arithmetic: 2.19 us -> 0 us
    unnamed x15 -> x0, local copies, waits for them, and re-layouts: 8.03 us -> none
    pallas_call x1 -> x2, Pallas kernels: 62.5 us -> 67 us  [the longest x1 65.3 us: body(): pl.pallas_call(functools.partial(kernel, sp, tp), in_specs=[hbm] * 7, out...]
    concatenate x2 -> x0, other arithmetic: 0.77 us -> none  [the longest x1 0.69 us: body(): jnp.concatenate([fold[:, 193:], jnp.sum(fold[:, :129], axis=1, keepdims=T...]
where the time goes in v1:
time: 67.8 us; the launch traced here: 67.6 us
  Pallas kernels  67 us (99%)
    pallas_call x1, Pallas kernels, body(): pl.pallas_call(functools.partial(kernel, sp, tp), in_specs=[hbm] * 7, out...  65.3 us
    pallas_call x1, Pallas kernels, body(): pl.pallas_call(drain, in_specs=[vmem] * 4, out_specs=[hbm] * 6, out_shape...  1.67 us

profile of v1, /device:TPU:0, one launch (start us, length us, event | category | flops | bytes accessed | tf_op | source)
XLA Modules:
  0.0 67.6 jit_solution(11347990547652688814)
XLA Ops:
  0.6 65.3 %attend.1 = (bf16[640,768]{1,0:T(8,128)(2,1)S(1)}, bf16[640,768]{1,0:T(8,128)(2,1)S(1)}, bf16[640,768]{1,0:T(8,128)(2,1)S(1)}, f32[7,8,128]{2,1,0:T(8,128)S(1)}) custom-call(bf16[640,768]{1,0:T(8,128)(2,1)} %q_hbm.1, bf16[640,768]{1,0:T(8,128)(2,1)} %k_hbm.1, bf16[640,768]{1,0:T(8,128)(2,1)} %v_hbm.1, bf16[640,768]{1,0:T(8,128)(2,1)} %g_hbm.1, ...), custom_call_target="tpu_custom_call" | custom-call | tf_op jit(solution)/shard_map/attend/pallas_call | solution.py:484
  65.9 1.7 %drain.1 = (bf16[640,768]{1,0:T(8,128)(2,1)}, bf16[640,768]{1,0:T(8,128)(2,1)}, bf16[640,768]{1,0:T(8,128)(2,1)}, f32[12,320]{1,0:T(8,128)}, f32[64]{0:T(128)}, /*index=5*/f32[64]{0:T(128)}) custom-call(bf16[640,768]{1,0:T(8,128)(2,1)S(1)} %get-tuple-element.10.qg_ref, bf16[640,768]{1,0:T(8,128)(2,1)S(1)} %get-tuple-element.11.kg_ref, ...), custom_call_target="tpu_custom_call" | custom-call | tf_op jit(solution)/shard_map/drain/pallas_call | solution.py:513

commit v2 on v1

--- a/solution.py
+++ b/solution.py
@@ -15,6 +15,7 @@
 BLK = 2 * SEG
 BAND = REACH + BLK
 NEG = -1e30
+LAG = 3
 F32 = jnp.float32
 BF16 = jnp.bfloat16
 
@@ -111,7 +112,7 @@
     sp, tp, q_hbm, k_hbm, v_hbm, g_hbm, qgain_hbm, kgain_hbm, table_hbm,
     qg_ref, kg_ref, vg_ref, out_ref,
     q_ref, k_ref, v_ref, g_ref,
-    k_s, kt_s, v_s, bias_s, acc_s, s_s, dw_s, ds_s, w_s, qs_s, gs_s, hat_s, scale_s, dk_s, dv_s, clip_s, gq_s, gk_s,
+    khat_s, k_s, kt_s, v_s, bias_s, acc_s, s_s, dw_s, ds_s, w_s, qs_s, gs_s, hat_s, scale_s, dk_s, dv_s, clip_s, gq_s, gk_s,
     pk_s, pv_s, ck_s, cv_s, bk_s, bv_s, bsum_s, bgot_s, gsum_s, ggot_s, gfirst_s,
     qgain_s, kgain_s, raw_s, wide_s, table_s, gains_s,
     prior_send, prior_recv, cross_send, cross_recv, bias_send, bias_recv, gain_send, gain_recv, load_sem, small_sem,
@@ -190,25 +191,22 @@
         bk_s[...] = jnp.zeros_like(bk_s)
         bv_s[...] = jnp.zeros_like(bv_s)
 
-    def bias_copies(r, p):
+    def bias_copies(p):
         return [
-            remote(bsum_s.at[r, p], bgot_s.at[r, p, k], bias_send.at[r, k, p], bias_recv.at[r, k, p], device)
+            remote(bsum_s.at[0, p], bgot_s.at[0, k, p], bias_send.at[0, k, p], bias_recv.at[0, k, p], device)
+            for k, device in enumerate(peers[0])
+        ]
+
+    def late_copies(r):
+        return [
+            remote(bsum_s.at[r], bgot_s.at[r, k], bias_send.at[r, k, 0], bias_recv.at[r, k, 0], device)
             for k, device in enumerate(peers[r])
         ]
 
-    def bias_start(r, p):
-        for copy in bias_copies(r, p):
-            copy.start()
-
-    def bias_add(r, p):
-        for copy in bias_copies(r, p):
+    def bias_add(r):
+        for copy in [copy for p in range(pairs) for copy in bias_copies(p)] if r == 0 else late_copies(r):
             copy.wait_recv()
-        bsum_s[r + 1, p] = ring_sum([bsum_s[r, p]] + [bgot_s[r, p, k] for k in range(len(peers[r]))])
-
-    def bias_step(r, p):
-        bias_add(r - 1, p)
-        if r < count:
-            bias_start(r, p)
+        bsum_s[r + 1] = ring_sum([bsum_s[r]] + [bgot_s[r, k] for k in range(len(peers[r]))])
 
     def gain_copies(r):
         if r == 0:
@@ -254,34 +252,33 @@
     gk_s[...] = jnp.zeros_like(gk_s)
 
     def key_tile(raw, b):
-        unit = normed(raw, ones)[0] * gain_k
+        hat = normed(raw, ones)[0]
+        khat_s[b * BLK : (b + 1) * BLK, :] = hat
+        unit = hat * gain_k
         k_s[b * BLK : (b + 1) * BLK, :] = unit.astype(BF16)
         kt_s[:, b * BLK : (b + 1) * BLK] = unit.T.astype(BF16)
 
-    def finish(p):
-        slot = lax.rem(p, 2)
+    def finish(p, _):
         @pl.when(jnp.logical_not(last))
         def _():
             for copy in cross_copies(p):
                 copy.wait_recv()
 
-        total = jnp.zeros((1, BLK), F32)
         for b in range(blocks):
             rows = slice(b * BLK, (b + 1) * BLK)
             hat, scale = normed(k_ref[rows, lanes_of(p)], ones)
             ext = slice(REACH + b * BLK, REACH + (b + 1) * BLK)
-            dk, dv = dk_s[slot, ext, :], dv_s[slot, ext, :]
+            dk, dv = dk_s[p, ext, :], dv_s[p, ext, :]
             back = b * BLK - (tokens - REACH)
             if back >= 0:
                 dk = dk + bk_s[p, back : back + BLK, :].astype(F32)
                 dv = dv + bv_s[p, back : back + BLK, :].astype(F32)
-            total = total + jnp.sum(dk * hat, axis=0, keepdims=True)
             kg_ref[rows, lanes_of(p)] = norm_grad(dk, gain_k, hat, scale, ones).astype(BF16)
             vg_ref[rows, lanes_of(p)] = dv.astype(BF16)
-        gk_s[...] += total
+        return 0
 
     def pair(p, _):
-        slot = lax.rem(p, 2)
+        slot = p
         for head in range(2):
             build_bias(table_s[pl.ds(p * 2 + head, 1), :], bias_s, head)
         dk_s[slot] = jnp.zeros(dk_s.shape[1:], F32)
@@ -370,6 +367,7 @@
                     w_s[here % 2, tile(j), :] = w.astype(BF16)
             if 0 <= here < blocks:
                 clip_s[...] += clipped
+        gk_s[...] += jnp.sum(dk_s[slot] * khat_s[...], axis=0, keepdims=True)
         ck_s[p] = dk_s[slot, :REACH, :].astype(BF16)
         cv_s[p] = dv_s[slot, :REACH, :].astype(BF16)
         @pl.when(jnp.logical_not(first))
@@ -384,32 +382,29 @@
             row = fold_bias(acc_s, head) + jnp.where(lane == 0, far, 0.0)
             rows += [row[:, b * BLK : (b + 1) * BLK] for b in range(4)]
         bsum_s[0, p] = jnp.concatenate(rows, axis=0)
-        bias_start(0, p)
-        for r in range(1, count + 1):
-
-            @pl.when(p >= r)
-            def _():
-                bias_step(r, p - r)
-
-        @pl.when(p > 0)
+        for copy in bias_copies(p):
+            copy.start()
+
+        @pl.when(p >= LAG)
         def _():
-            finish(p - 1)
+            finish(p - LAG, 0)
 
         return 0
 
     lax.fori_loop(0, pairs, pair, 0)
-    finish(pairs - 1)
     gsum_s[0] = jnp.zeros(gsum_s.shape[1:], F32)
     gsum_s[0, 0:1, :] = gq_s[...]
     gsum_s[0, 1:2, :] = gk_s[...]
     gain_start(0)
-    for t in range(count):
-        for r in range(1, count + 1):
-            if 0 <= pairs + t - r < pairs:
-                bias_step(r, pairs + t - r)
-        gain_add(t)
-        if t + 1 < count:
-            gain_start(t + 1)
+    for r in range(count):
+        bias_add(r)
+        if r + 1 < count:
+            for copy in late_copies(r + 1):
+                copy.start()
+        gain_add(r)
+        if r + 1 < count:
+            gain_start(r + 1)
+    lax.fori_loop(max(pairs - LAG, 0), pairs, finish, 0)
     for p in range(pairs):
         out_ref[p] = bsum_s[count, p]
     out_ref[pairs] = gsum_s[count]
@@ -427,9 +422,8 @@
                 copy.wait_send()
 
     for r in range(count):
-        for p in range(pairs):
-            for copy in bias_copies(r, p):
-                copy.wait_send()
+        for copy in [copy for p in range(pairs) for copy in bias_copies(p)] if r == 0 else late_copies(r):
+            copy.wait_send()
         for copy in gain_copies(r):
             copy.wait_send()
 
@@ -488,18 +482,19 @@
         out_shape=[grads, grads, grads, shape((pairs + 1, 8, BLK), F32)],
         scratch_shapes=[pltpu.VMEM((tokens, heads * 64), BF16)] * 4
         + [
+            pltpu.VMEM((ext, BLK), F32),
             pltpu.VMEM((ext, BLK), BF16), pltpu.VMEM((BLK, ext), BF16), pltpu.VMEM((ext, BLK), BF16),
             pltpu.VMEM((BAND, 2 * BLK), F32), pltpu.VMEM((3 * BLK, 2 * BLK), F32),
             pltpu.VMEM((2, BAND, 2 * BLK), F32), pltpu.VMEM((2, BAND, 2 * BLK), F32),
             pltpu.VMEM((2, BAND, 2 * BLK), BF16), pltpu.VMEM((2, BAND, 2 * BLK), BF16),
             pltpu.VMEM((tokens // BLK, 2 * BLK, BLK), BF16), pltpu.VMEM((tokens // BLK, 2 * BLK, BLK), BF16),
             pltpu.VMEM((tokens, BLK), F32), pltpu.VMEM((tokens, BLK), F32),
-            pltpu.VMEM((2, ext, BLK), F32), pltpu.VMEM((2, ext, BLK), F32),
+            pltpu.VMEM((pairs, ext, BLK), F32), pltpu.VMEM((pairs, ext, BLK), F32),
             pltpu.VMEM((1, 2 * BLK), F32), pltpu.VMEM((1, BLK), F32), pltpu.VMEM((1, BLK), F32),
         ]
         + [pltpu.VMEM((pairs, REACH, BLK), BF16)] * 6
         + [
-            pltpu.VMEM((count + 1, pairs, 8, BLK), F32), pltpu.VMEM((count, pairs, 3, 8, BLK), F32),
+            pltpu.VMEM((count + 1, pairs, 8, BLK), F32), pltpu.VMEM((count, 3, pairs, 8, BLK), F32),
             pltpu.VMEM((count + 1, 8, BLK), F32), pltpu.VMEM((count, 3, 8, BLK), F32), pltpu.VMEM((group, 8, BLK), F32),
             pltpu.VMEM((1, 64), BF16), pltpu.VMEM((1, 64), BF16), pltpu.VMEM(position_bias.shape, BF16),
             pltpu.VMEM((padded, 512), F32), pltpu.VMEM((padded, 512), F32), pltpu.VMEM((8, BLK), F32),

time: 67.8 us -> 58.2 us (0.86)
  Pallas kernels: 67 us -> 57.4 us
    pallas_call x1, Pallas kernels: 65.3 us -> 55.7 us  [body(): pl.pallas_call(functools.partial(kernel, sp, tp), in_specs=[hbm] * 7, out...]
where the time goes in v2:
time: 58.2 us; the launch traced here: 58 us
  Pallas kernels  57.4 us (99%)
  between operations  0.64 us (1%)
    pallas_call x1, Pallas kernels, body(): pl.pallas_call(functools.partial(kernel, sp, tp), in_specs=[hbm] * 7, out...  55.7 us
    pallas_call x1, Pallas kernels, body(): pl.pallas_call(drain, in_specs=[vmem] * 4, out_specs=[hbm] * 6, out_shape...  1.67 us

profile of v2, /device:TPU:0, one launch (start us, length us, event | category | flops | bytes accessed | tf_op | source)
XLA Modules:
  0.0 58.0 jit_solution(9656346347464686308)
XLA Ops:
  0.6 55.7 %attend.1 = (bf16[640,768]{1,0:T(8,128)(2,1)S(1)}, bf16[640,768]{1,0:T(8,128)(2,1)S(1)}, bf16[640,768]{1,0:T(8,128)(2,1)S(1)}, f32[7,8,128]{2,1,0:T(8,128)S(1)}) custom-call(bf16[640,768]{1,0:T(8,128)(2,1)} %q_hbm.1, bf16[640,768]{1,0:T(8,128)(2,1)} %k_hbm.1, bf16[640,768]{1,0:T(8,128)(2,1)} %v_hbm.1, bf16[640,768]{1,0:T(8,128)(2,1)} %g_hbm.1, ...), custom_call_target="tpu_custom_call" | custom-call | tf_op jit(solution)/shard_map/attend/pallas_call | solution.py:478
  56.3 1.7 %drain.1 = (bf16[640,768]{1,0:T(8,128)(2,1)}, bf16[640,768]{1,0:T(8,128)(2,1)}, bf16[640,768]{1,0:T(8,128)(2,1)}, f32[12,320]{1,0:T(8,128)}, f32[64]{0:T(128)}, /*index=5*/f32[64]{0:T(128)}) custom-call(bf16[640,768]{1,0:T(8,128)(2,1)S(1)} %get-tuple-element.10.qg_ref, bf16[640,768]{1,0:T(8,128)(2,1)S(1)} %get-tuple-element.11.kg_ref, ...), custom_call_target="tpu_custom_call" | custom-call | tf_op jit(solution)/shard_map/drain/pallas_call | solution.py:508

commit v3 on v2

--- a/solution.py
+++ b/solution.py
@@ -15,7 +15,10 @@
 BLK = 2 * SEG
 BAND = REACH + BLK
 NEG = -1e30
-LAG = 3
+LAG = 2
+AHEAD = 2
+PART = 32
+EARLY = 2
 F32 = jnp.float32
 BF16 = jnp.bfloat16
 
@@ -25,15 +28,15 @@
 
 
 def half_ones():
-    row = lax.broadcasted_iota(jnp.int32, (BLK, BLK), 0) // 64
-    col = lax.broadcasted_iota(jnp.int32, (BLK, BLK), 1) // 64
+    row = lax.broadcasted_iota(jnp.int32, (2 * BLK, BLK), 0) // 64 % 2
+    col = lax.broadcasted_iota(jnp.int32, (2 * BLK, BLK), 1) // 64
     return jnp.where(row == col, 1.0, 0.0).astype(BF16)
 
 
 def head_mean(x, ones):
     high = x.astype(BF16)
     low = (x - high.astype(F32)).astype(BF16)
-    return (dot(high, ones, ((1,), (0,))) + dot(low, ones, ((1,), (0,)))) * (1.0 / 64.0)
+    return dot(jnp.concatenate([high, low], axis=1), ones, ((1,), (0,))) * (1.0 / 64.0)
 
 
 def normed(rows, ones):
@@ -88,6 +91,10 @@
     return wide[0:1]
 
 
+def grouped(x):
+    return x.reshape(x.shape[0] // 8, 8, x.shape[1])
+
+
 def rounds_of(size):
     rounds, stride = [], 1
     while stride < size:
@@ -112,14 +119,22 @@
     sp, tp, q_hbm, k_hbm, v_hbm, g_hbm, qgain_hbm, kgain_hbm, table_hbm,
     qg_ref, kg_ref, vg_ref, out_ref,
     q_ref, k_ref, v_ref, g_ref,
-    khat_s, k_s, kt_s, v_s, bias_s, acc_s, s_s, dw_s, ds_s, w_s, qs_s, gs_s, hat_s, scale_s, dk_s, dv_s, clip_s, gq_s, gk_s,
-    pk_s, pv_s, ck_s, cv_s, bk_s, bv_s, bsum_s, bgot_s, gsum_s, ggot_s, gfirst_s,
+    k_s, kt_s, qs_s, gs_s, khat_s, kscale_s, qhat_s, qscale_s, nhat_s, dq_s,
+    bias_s, acc_s, clip_s, e_s, dw_s, peak_s, factor_s, delta_s, ds_s, w_s, gq_s, gk_s,
+    nq_s, ng_s, cq_s, bq_s, mid_s, own_s, next_s, before_s, after_s,
+    bsum_s, bgot_s, gsum_s, ggot_s, gfirst_s,
     qgain_s, kgain_s, raw_s, wide_s, table_s, gains_s,
-    prior_send, prior_recv, cross_send, cross_recv, bias_send, bias_recv, gain_send, gain_recv, load_sem, small_sem,
+    rows_send, rows_recv, back_send, back_recv, part_send, part_recv,
+    bias_send, bias_recv, gain_send, gain_recv, load_sem, small_sem,
 ):
     tokens = q_ref.shape[0]
     blocks = tokens // BLK
-    pairs = pk_s.shape[0]
+    cross = REACH // BLK
+    pairs = nq_s.shape[0]
+    tiles = {}
+    for qb in range(blocks + cross):
+        for kb in range(max(qb - cross, 0), min(qb + 1, blocks)):
+            tiles[qb, kb] = len(tiles)
     me = lax.axis_index("sp")
     me_tp = lax.axis_index("tp")
     right, left = lax.rem(me + 1, sp), lax.rem(me + sp - 1, sp)
@@ -129,6 +144,13 @@
     combos = [(k, t) for k in range(rounds[0][1]) for t in range(tp) if k or t]
     nearby = [{"sp": peer(me, 1, rounds[0][1], k), "tp": lax.rem(me_tp + t, tp)} for k, t in combos]
     first, last = me == 0, me == sp - 1
+    has_left, has_right = jnp.logical_not(first), jnp.logical_not(last)
+
+    def tile(j):
+        return slice(j * BLK, (j + 1) * BLK)
+
+    def wide_tile(j):
+        return slice(j * 2 * BLK, (j + 1) * 2 * BLK)
 
     def lanes_of(p):
         return pl.ds(pl.multiple_of(p * BLK, BLK), BLK)
@@ -162,34 +184,43 @@
             device_id=device, device_id_type=pl.DeviceIdType.MESH,
         )
 
-    def prior_copies(p):
-        rows = slice(tokens - REACH, tokens)
+    def row_copies(p):
+        rows = slice(0, REACH)
         return (
-            remote(k_hbm.at[rows, lanes_of(p)], pk_s.at[p], prior_send.at[0, p], prior_recv.at[0, p], {"sp": right}),
-            remote(v_hbm.at[rows, lanes_of(p)], pv_s.at[p], prior_send.at[1, p], prior_recv.at[1, p], {"sp": right}),
+            remote(q_hbm.at[rows, lanes_of(p)], nq_s.at[p], rows_send.at[0, p], rows_recv.at[0, p], {"sp": left}),
+            remote(g_hbm.at[rows, lanes_of(p)], ng_s.at[p], rows_send.at[1, p], rows_recv.at[1, p], {"sp": left}),
         )
 
-    def cross_copies(p):
-        return (
-            remote(ck_s.at[p], bk_s.at[p], cross_send.at[0, p], cross_recv.at[0, p], {"sp": left}),
-            remote(cv_s.at[p], bv_s.at[p], cross_send.at[1, p], cross_recv.at[1, p], {"sp": left}),
-        )
-
-    @pl.when(jnp.logical_not(last))
+    def back_copy(p):
+        return remote(cq_s.at[p], bq_s.at[p], back_send.at[p], back_recv.at[p], {"sp": right})
+
+    def own_copy(p):
+        return remote(own_s.at[p], after_s.at[p], part_send.at[0, p], part_recv.at[0, p], {"sp": left})
+
+    def next_copy(p):
+        return remote(next_s.at[p], before_s.at[p], part_send.at[1, p], part_recv.at[1, p], {"sp": right})
+
+    @pl.when(has_left)
     def _():
-        for p in range(pairs):
-            for copy in prior_copies(p):
+        for p in range(min(AHEAD, pairs)):
+            for copy in row_copies(p):
                 copy.start()
 
     @pl.when(first)
     def _():
-        pk_s[...] = jnp.zeros_like(pk_s)
-        pv_s[...] = jnp.zeros_like(pv_s)
+        bq_s[...] = jnp.zeros_like(bq_s)
+        before_s[...] = jnp.zeros_like(before_s)
+        for p in range(pairs):
+            before_s[p, 0:cross, :] = jnp.full((cross, 2 * BLK), NEG, F32)
 
     @pl.when(last)
     def _():
-        bk_s[...] = jnp.zeros_like(bk_s)
-        bv_s[...] = jnp.zeros_like(bv_s)
+        nq_s[...] = jnp.zeros_like(nq_s)
+        ng_s[...] = jnp.zeros_like(ng_s)
+        after_s[...] = jnp.zeros_like(after_s)
+        for p in range(pairs):
+            after_s[p, 0:cross, :] = jnp.full((cross, 2 * BLK), -NEG, F32)
+            after_s[p, cross : 2 * cross, :] = jnp.ones((cross, 2 * BLK), F32)
 
     def bias_copies(p):
         return [
@@ -251,147 +282,261 @@
     gq_s[...] = jnp.zeros_like(gq_s)
     gk_s[...] = jnp.zeros_like(gk_s)
 
-    def key_tile(raw, b):
-        hat = normed(raw, ones)[0]
-        khat_s[b * BLK : (b + 1) * BLK, :] = hat
-        unit = hat * gain_k
-        k_s[b * BLK : (b + 1) * BLK, :] = unit.astype(BF16)
-        kt_s[:, b * BLK : (b + 1) * BLK] = unit.T.astype(BF16)
-
-    def finish(p, _):
-        @pl.when(jnp.logical_not(last))
-        def _():
-            for copy in cross_copies(p):
+    def query_tile(slot, qb, raw, grad):
+        hat, scale = normed(raw, ones)
+        qs_s[slot, wide_tile(qb), :] = stack_halves((hat * gain_q).astype(BF16) * jnp.asarray(0.125, BF16))
+        gs_s[slot, wide_tile(qb), :] = stack_halves(grad)
+        return hat, scale
+
+    def scores(p, slot, qb):
+        peaks, sums, deltas = [], [], []
+        for kb in range(max(qb - cross, 0), min(qb + 1, blocks)):
+            place = tiles[qb, kb]
+            j = kb - qb + cross
+            s = dot(k_s[slot, tile(kb), :], qs_s[slot, wide_tile(qb), :], ((1,), (1,))) + bias_s[tile(j), :]
+            s = grouped(s)
+            peak = jnp.max(s, axis=0)
+            e = jnp.exp(s - peak[None])
+            dw = dot(v_ref[tile(kb), lanes_of(p)], gs_s[slot, wide_tile(qb), :], ((1,), (1,)))
+            e_s[slot, place] = e.reshape(BLK, 2 * BLK)
+            dw_s[slot, place] = dw
+            peak_s[slot, place] = peak
+            peaks.append(peak)
+            sums.append(jnp.sum(e, axis=0))
+            deltas.append(jnp.sum(e * grouped(dw), axis=0))
+        peak = jnp.max(functools.reduce(jnp.maximum, peaks), axis=0, keepdims=True)
+        total = jnp.zeros((8, 2 * BLK), F32)
+        delta = jnp.zeros((8, 2 * BLK), F32)
+        for part, a, b in zip(peaks, sums, deltas):
+            factor = jnp.exp(part - peak)
+            total = total + a * factor
+            delta = delta + b * factor
+        found = (peak, jnp.sum(total, axis=0, keepdims=True), jnp.sum(delta, axis=0, keepdims=True))
+        for n, row in enumerate(found):
+            if qb < cross:
+                own_s[p, n * cross + qb : n * cross + qb + 1, :] = row
+            elif qb < blocks:
+                mid_s[slot, n : n + 1, :] = row
+            else:
+                at = n * cross + qb - blocks
+                next_s[p, at : at + 1, :] = row
+
+    def forward(p):
+        slot = lax.rem(p, 2)
+        for copy in loads(p):
+            copy.wait()
+
+        def prepare(b):
+            hat, scale = normed(k_ref[tile(b), lanes_of(p)], ones)
+            khat_s[slot, tile(b), :] = hat
+            kscale_s[slot, tile(b), :] = scale
+            unit = hat * gain_k
+            k_s[slot, tile(b), :] = unit.astype(BF16)
+            kt_s[lax.rem(p, 3), :, tile(b)] = unit.T.astype(BF16)
+            hat, scale = query_tile(slot, b, q_ref[tile(b), lanes_of(p)], g_ref[tile(b), lanes_of(p)])
+            qhat_s[p, tile(b), :] = hat
+            qscale_s[p, tile(b), :] = scale
+
+        past = jnp.maximum(p - 2, 0)
+        for b in range(EARLY):
+            prepare(b)
+        for b in range(blocks):
+            if b + EARLY < blocks:
+                prepare(b + EARLY)
+            rest_query(past, b, p >= 2)
+            scores(p, slot, b)
+        rest_bias(past)
+
+        @pl.when(p >= 2)
+        def _():
+            for copy in bias_copies(past):
+                copy.start()
+
+        @pl.when(has_left)
+        def _():
+            own_copy(p).start()
+
+        @pl.when(has_left & (p + AHEAD < pairs))
+        def _():
+            for copy in row_copies(p + AHEAD):
+                copy.start()
+
+        @pl.when(has_right)
+        def _():
+            for copy in row_copies(p):
                 copy.wait_recv()
 
-        for b in range(blocks):
-            rows = slice(b * BLK, (b + 1) * BLK)
-            hat, scale = normed(k_ref[rows, lanes_of(p)], ones)
-            ext = slice(REACH + b * BLK, REACH + (b + 1) * BLK)
-            dk, dv = dk_s[p, ext, :], dv_s[p, ext, :]
-            back = b * BLK - (tokens - REACH)
-            if back >= 0:
-                dk = dk + bk_s[p, back : back + BLK, :].astype(F32)
-                dv = dv + bv_s[p, back : back + BLK, :].astype(F32)
-            kg_ref[rows, lanes_of(p)] = norm_grad(dk, gain_k, hat, scale, ones).astype(BF16)
-            vg_ref[rows, lanes_of(p)] = dv.astype(BF16)
-        return 0
-
-    def pair(p, _):
-        slot = p
+        for b in range(cross):
+            hat, _ = query_tile(slot, blocks + b, nq_s[p, tile(b), :], ng_s[p, tile(b), :])
+            nhat_s[slot, tile(b), :] = hat
+        for b in range(cross):
+            scores(p, slot, blocks + b)
+
+        @pl.when(has_right)
+        def _():
+            next_copy(p).start()
+
+    def next_bias(p):
         for head in range(2):
             build_bias(table_s[pl.ds(p * 2 + head, 1), :], bias_s, head)
-        dk_s[slot] = jnp.zeros(dk_s.shape[1:], F32)
-        dv_s[slot] = jnp.zeros(dv_s.shape[1:], F32)
-        acc_s[...] = jnp.zeros_like(acc_s)
-        clip_s[...] = jnp.zeros_like(clip_s)
-        for copy in loads(p):
-            copy.wait()
-        for b in range(blocks):
-            rows = slice(b * BLK, (b + 1) * BLK)
-            key_tile(k_ref[rows, lanes_of(p)], b + LEFT // 2)
-            hat, scale = normed(q_ref[rows, lanes_of(p)], ones)
-            hat_s[rows, :] = hat
-            scale_s[rows, :] = scale
-            qs_s[b] = stack_halves((hat * gain_q).astype(BF16) * jnp.asarray(0.125, BF16))
-            gs_s[b] = stack_halves(g_ref[rows, lanes_of(p)])
-        v_s[REACH:, :] = v_ref[:, lanes_of(p)]
-        @pl.when(jnp.logical_not(first))
-        def _():
-            for copy in prior_copies(p):
-                copy.wait_recv()
-
-        for b in range(LEFT // 2):
-            key_tile(pk_s[p, b * BLK : (b + 1) * BLK, :], b)
-        v_s[:REACH, :] = pv_s[p]
-
-        def tile(j):
-            return slice(j * BLK, (j + 1) * BLK)
-
-        def score(i, j, peaks):
-            keys = tile(i + j)
-            s = dot(k_s[keys, :], qs_s[i], ((1,), (1,))) + bias_s[tile(j), :]
-            s_s[i % 2, tile(j), :] = s
-            dw_s[i % 2, tile(j), :] = dot(v_s[keys, :], gs_s[i], ((1,), (1,)))
-            top = jnp.max(s, axis=0, keepdims=True)
-            peaks.append(top + penalty if j < LEFT // 2 - i else top)
-
-        def product(i, j):
-            keys = tile(i + j)
-            dk_s[slot, keys, :] += dot(ds_s[i % 2, tile(j), :], qs_s[i], ((1,), (0,)))
-            dv_s[slot, keys, :] += dot(w_s[i % 2, tile(j), :], gs_s[i], ((1,), (0,)))
-
-        def query_side(i):
-            rows = tile(i)
-            dqt = dot(kt_s[:, i * BLK : i * BLK + BAND], ds_s[i % 2], ((1,), (0,)))
-            dqt = jnp.concatenate([dqt[:64, :BLK], dqt[64:, BLK:]], axis=0)
-            dq = dqt.T * 0.125
-            hat = hat_s[rows, :]
-            gq_s[...] += jnp.sum(dq * hat, axis=0, keepdims=True)
-            qg_ref[rows, lanes_of(p)] = norm_grad(dq, gain_q, hat, scale_s[rows, :], ones).astype(BF16)
-
-        penalty = jnp.where(first, NEG, 0.0)
-        peaks = {}
-        for step in range(blocks + 2):
-            ahead, here, behind = step, step - 1, step - 2
-            peaks[ahead] = []
-            if 0 <= here < blocks:
-                peak = functools.reduce(jnp.maximum, peaks[here])
-                total = jnp.zeros((1, 2 * BLK), F32)
-                delta = jnp.zeros((1, 2 * BLK), F32)
-                clipped = jnp.zeros((1, 2 * BLK), F32)
-            for j in range(5):
-                if ahead < blocks:
-                    score(ahead, j, peaks[ahead])
-                if 0 <= here < blocks:
-                    e = jnp.exp(s_s[here % 2, tile(j), :] - (peak - penalty if j < LEFT // 2 - here else peak))
-                    s_s[here % 2, tile(j), :] = e
-                    total = total + jnp.sum(e, axis=0, keepdims=True)
-                    delta = delta + jnp.sum(e * dw_s[here % 2, tile(j), :], axis=0, keepdims=True)
-            if 0 <= here < blocks:
-                inverse = 1.0 / total
-                delta = delta * inverse
-            if behind >= 0:
-                query_side(behind)
-            for j in range(5):
-                if behind >= 0:
-                    product(behind, j)
-                if 0 <= here < blocks:
-                    w = s_s[here % 2, tile(j), :] * inverse
-                    ds = w * (dw_s[here % 2, tile(j), :] - delta)
+
+    def settle(mine, other):
+        here, there = mine[:cross], other[:cross]
+        peak = jnp.maximum(here, there)
+        a, b = jnp.exp(here - peak), jnp.exp(there - peak)
+        total = mine[cross : 2 * cross] * a + other[cross : 2 * cross] * b
+        delta = mine[2 * cross : 3 * cross] * a + other[2 * cross : 3 * cross] * b
+        inverse = 1.0 / total
+        return peak, inverse, delta * inverse
+
+    def backward(p):
+        slot = lax.rem(p, 2)
+
+        @pl.when(has_left)
+        def _():
+            next_copy(p).wait_recv()
+
+        @pl.when(has_right)
+        def _():
+            own_copy(p).wait_recv()
+
+        own = settle(own_s[p], before_s[p])
+        later = settle(next_s[p], after_s[p])
+        inverse = 1.0 / mid_s[slot, 1:2, :]
+        mid = (mid_s[slot, 0:1, :], inverse, mid_s[slot, 2:3, :] * inverse)
+        for qb in range(blocks + cross):
+            found, at = (own, qb) if qb < cross else (mid, 0) if qb < blocks else (later, qb - blocks)
+            peak, inverse, delta = (x[at : at + 1] for x in found)
+            delta_s[qb] = jnp.broadcast_to(delta, (8, 2 * BLK))
+            for kb in range(max(qb - cross, 0), min(qb + 1, blocks)):
+                place = tiles[qb, kb]
+                factor_s[place] = jnp.exp(peak_s[slot, place] - peak) * inverse
+
+        clipped = jnp.zeros((8, 2 * BLK), F32)
+        gain_sum = jnp.zeros((1, BLK), F32)
+        for kb in reversed(range(blocks)):
+            for qb in range(kb, kb + cross + 1):
+                place, j = tiles[qb, kb], kb - qb + cross
+                for part in range(BLK // PART):
+                    rows = slice(part * PART, (part + 1) * PART)
+                    w = grouped(e_s[slot, place, rows, :]) * factor_s[place][None]
+                    ds = w * (grouped(dw_s[slot, place, rows, :]) - delta_s[qb][None])
                     if j < 2:
-                        clipped = clipped + jnp.sum(ds, axis=0, keepdims=True)
-                    else:
-                        acc_s[tile(j - 2), :] += ds
-                    ds_s[here % 2, tile(j), :] = ds.astype(BF16)
-                    w_s[here % 2, tile(j), :] = w.astype(BF16)
-            if 0 <= here < blocks:
-                clip_s[...] += clipped
-        gk_s[...] += jnp.sum(dk_s[slot] * khat_s[...], axis=0, keepdims=True)
-        ck_s[p] = dk_s[slot, :REACH, :].astype(BF16)
-        cv_s[p] = dv_s[slot, :REACH, :].astype(BF16)
-        @pl.when(jnp.logical_not(first))
-        def _():
-            for copy in cross_copies(p):
-                copy.start()
-
+                        clipped = clipped + jnp.sum(ds, axis=0)
+                    ds, w = ds.reshape(PART, 2 * BLK), w.reshape(PART, 2 * BLK)
+                    if j >= 2:
+                        at = slice((j - 2) * BLK + part * PART, (j - 2) * BLK + (part + 1) * PART)
+                        acc_s[at, :] = ds if kb == blocks - 1 else acc_s[at, :] + ds
+                    at = slice(kb * BLK + part * PART, kb * BLK + (part + 1) * PART)
+                    ds_s[at, wide_tile(qb)] = ds.astype(BF16)
+                    w_s[at, wide_tile(qb)] = w.astype(BF16)
+            inner = slice(kb * 2 * BLK, blocks * 2 * BLK)
+            outer = slice(blocks * 2 * BLK, (kb + cross + 1) * 2 * BLK)
+            dk = dot(ds_s[tile(kb), inner], qs_s[slot, inner, :], ((1,), (0,)))
+            dv = dot(w_s[tile(kb), inner], gs_s[slot, inner, :], ((1,), (0,)))
+            if kb + cross >= blocks:
+                dk = dk + dot(ds_s[tile(kb), outer], qs_s[slot, outer, :], ((1,), (0,))).astype(BF16).astype(F32)
+                dv = dv + dot(w_s[tile(kb), outer], gs_s[slot, outer, :], ((1,), (0,))).astype(BF16).astype(F32)
+            hat = khat_s[slot, tile(kb), :]
+            gain_sum = gain_sum + jnp.sum(dk * hat, axis=0, keepdims=True)
+            kg_ref[tile(kb), lanes_of(p)] = norm_grad(dk, gain_k, hat, kscale_s[slot, tile(kb), :], ones).astype(BF16)
+            vg_ref[tile(kb), lanes_of(p)] = dv.astype(BF16)
+            if kb > 0:
+                query_side(p, slot, kb + cross)
+        gk_s[...] += gain_sum
+        clip_s[...] = clipped
+        next_bias(jnp.minimum(p + 2, pairs - 1))
+
+        @pl.when(has_right)
+        def _():
+            back_copy(p).start()
+
+    def turned(p, qb):
+        keys = slice(max(qb - cross, 0) * BLK, min(qb + 1, blocks) * BLK)
+        dqt = dot(kt_s[lax.rem(p, 3), :, keys], ds_s[keys, wide_tile(qb)], ((1,), (0,)))
+        dqt = jnp.concatenate([dqt[:64, :BLK], dqt[64:, BLK:]], axis=0)
+        return dqt.T * 0.125
+
+    def query_side(p, slot, qb):
+        dq = turned(p, qb)
+        cq_s[p, tile(qb - blocks), :] = dq.astype(BF16)
+        gq_s[...] += jnp.sum(dq * nhat_s[slot, tile(qb - blocks), :], axis=0, keepdims=True)
+
+    def rest_query(p, qb, live):
+        dq = turned(p, qb)
+        dq_s[p, tile(qb), :] = dq
+        part = jnp.sum(dq * qhat_s[p, tile(qb), :], axis=0, keepdims=True)
+        gq_s[...] += jnp.where(live, part, 0.0)
+
+    def rest_bias(p):
         lane = lax.broadcasted_iota(jnp.int32, (1, 512), 1)
         rows = []
+        clipped = jnp.sum(clip_s[...], axis=0, keepdims=True)
         for head in range(2):
-            far = jnp.sum(clip_s[:, head * BLK : (head + 1) * BLK], axis=1, keepdims=True)
+            far = jnp.sum(clipped[:, head * BLK : (head + 1) * BLK], axis=1, keepdims=True)
             row = fold_bias(acc_s, head) + jnp.where(lane == 0, far, 0.0)
             rows += [row[:, b * BLK : (b + 1) * BLK] for b in range(4)]
         bsum_s[0, p] = jnp.concatenate(rows, axis=0)
+
+    def rest(p):
+        for qb in range(blocks):
+            rest_query(p, qb, True)
+        rest_bias(p)
         for copy in bias_copies(p):
             copy.start()
 
-        @pl.when(p >= LAG)
-        def _():
-            finish(p - LAG, 0)
-
+    def finish(p, _):
+        @pl.when(has_left)
+        def _():
+            back_copy(p).wait_recv()
+
+        for b in range(blocks):
+            dq = dq_s[p, tile(b), :]
+            if b < cross:
+                dq = dq + bq_s[p, tile(b), :].astype(F32)
+            grad = norm_grad(dq, gain_q, qhat_s[p, tile(b), :], qscale_s[p, tile(b), :], ones)
+            qg_ref[tile(b), lanes_of(p)] = grad.astype(BF16)
+
+        @pl.when(has_left)
+        def _():
+            for copy in (*row_copies(p), own_copy(p)):
+                copy.wait_send()
+
+        @pl.when(has_right)
+        def _():
+            for copy in (back_copy(p), next_copy(p)):
+                copy.wait_send()
+
+        for copy in bias_copies(p):
+            copy.wait_send()
         return 0
 
-    lax.fori_loop(0, pairs, pair, 0)
+    def step(t, _):
+        @pl.when(t < pairs)
+        def _():
+            forward(t)
+
+        @pl.when(t == pairs)
+        def _():
+            rest(pairs - 2)
+
+        @pl.when(t == 0)
+        def _():
+            next_bias(min(1, pairs - 1))
+
+        @pl.when(t >= 1)
+        def _():
+            backward(t - 1)
+
+        @pl.when(t >= 1 + LAG)
+        def _():
+            finish(t - 1 - LAG, 0)
+
+        return 0
+
+    next_bias(0)
+    lax.fori_loop(0, pairs + 1, step, 0)
+    rest(pairs - 1)
     gsum_s[0] = jnp.zeros(gsum_s.shape[1:], F32)
     gsum_s[0, 0:1, :] = gq_s[...]
     gsum_s[0, 1:2, :] = gk_s[...]
@@ -409,21 +554,10 @@
         out_ref[p] = bsum_s[count, p]
     out_ref[pairs] = gsum_s[count]
 
-    @pl.when(jnp.logical_not(last))
-    def _():
-        for p in range(pairs):
-            for copy in prior_copies(p):
+    for r in range(count):
+        if r > 0:
+            for copy in late_copies(r):
                 copy.wait_send()
-
-    @pl.when(jnp.logical_not(first))
-    def _():
-        for p in range(pairs):
-            for copy in cross_copies(p):
-                copy.wait_send()
-
-    for r in range(count):
-        for copy in [copy for p in range(pairs) for copy in bias_copies(p)] if r == 0 else late_copies(r):
-            copy.wait_send()
         for copy in gain_copies(r):
             copy.wait_send()
 
@@ -466,6 +600,7 @@
     count = len(rounds_of(sp))
     group = 4 * tp
     ext = tokens + REACH
+    held = (REACH // BLK + 1) * (tokens // BLK)
     padded = (heads + 7) // 8 * 8
     vmem, hbm = pl.BlockSpec(memory_space=pltpu.VMEM), pl.BlockSpec(memory_space=pltpu.HBM)
     shape = jax.ShapeDtypeStruct
@@ -482,23 +617,27 @@
         out_shape=[grads, grads, grads, shape((pairs + 1, 8, BLK), F32)],
         scratch_shapes=[pltpu.VMEM((tokens, heads * 64), BF16)] * 4
         + [
-            pltpu.VMEM((ext, BLK), F32),
-            pltpu.VMEM((ext, BLK), BF16), pltpu.VMEM((BLK, ext), BF16), pltpu.VMEM((ext, BLK), BF16),
-            pltpu.VMEM((BAND, 2 * BLK), F32), pltpu.VMEM((3 * BLK, 2 * BLK), F32),
-            pltpu.VMEM((2, BAND, 2 * BLK), F32), pltpu.VMEM((2, BAND, 2 * BLK), F32),
-            pltpu.VMEM((2, BAND, 2 * BLK), BF16), pltpu.VMEM((2, BAND, 2 * BLK), BF16),
-            pltpu.VMEM((tokens // BLK, 2 * BLK, BLK), BF16), pltpu.VMEM((tokens // BLK, 2 * BLK, BLK), BF16),
-            pltpu.VMEM((tokens, BLK), F32), pltpu.VMEM((tokens, BLK), F32),
-            pltpu.VMEM((pairs, ext, BLK), F32), pltpu.VMEM((pairs, ext, BLK), F32),
-            pltpu.VMEM((1, 2 * BLK), F32), pltpu.VMEM((1, BLK), F32), pltpu.VMEM((1, BLK), F32),
+            pltpu.VMEM((2, tokens, BLK), BF16), pltpu.VMEM((3, BLK, tokens), BF16),
+            pltpu.VMEM((2, ext * 2, BLK), BF16), pltpu.VMEM((2, ext * 2, BLK), BF16),
+            pltpu.VMEM((2, tokens, BLK), F32), pltpu.VMEM((2, tokens, BLK), F32),
+            pltpu.VMEM((pairs, tokens, BLK), F32), pltpu.VMEM((pairs, tokens, BLK), F32),
+            pltpu.VMEM((2, REACH, BLK), F32), pltpu.VMEM((pairs, tokens, BLK), F32),
+            pltpu.VMEM((BAND, 2 * BLK), F32), pltpu.VMEM((3 * BLK, 2 * BLK), F32), pltpu.VMEM((8, 2 * BLK), F32),
+            pltpu.VMEM((2, held, BLK, 2 * BLK), F32), pltpu.VMEM((2, held, BLK, 2 * BLK), F32),
+            pltpu.VMEM((2, held, 8, 2 * BLK), F32), pltpu.VMEM((held, 8, 2 * BLK), F32),
+            pltpu.VMEM((ext // BLK, 8, 2 * BLK), F32),
+            pltpu.VMEM((tokens, ext * 2), BF16), pltpu.VMEM((tokens, ext * 2), BF16),
+            pltpu.VMEM((1, BLK), F32), pltpu.VMEM((1, BLK), F32),
         ]
-        + [pltpu.VMEM((pairs, REACH, BLK), BF16)] * 6
+        + [pltpu.VMEM((pairs, REACH, BLK), BF16)] * 4
+        + [pltpu.VMEM((2, 8, 2 * BLK), F32)]
+        + [pltpu.VMEM((pairs, 16, 2 * BLK), F32)] * 4
         + [
             pltpu.VMEM((count + 1, pairs, 8, BLK), F32), pltpu.VMEM((count, 3, pairs, 8, BLK), F32),
             pltpu.VMEM((count + 1, 8, BLK), F32), pltpu.VMEM((count, 3, 8, BLK), F32), pltpu.VMEM((group, 8, BLK), F32),
             pltpu.VMEM((1, 64), BF16), pltpu.VMEM((1, 64), BF16), pltpu.VMEM(position_bias.shape, BF16),
             pltpu.VMEM((padded, 512), F32), pltpu.VMEM((padded, 512), F32), pltpu.VMEM((8, BLK), F32),
-            sems((2, pairs)), sems((2, pairs)), sems((2, pairs)), sems((2, pairs)),
+            sems((2, pairs)), sems((2, pairs)), sems((pairs,)), sems((pairs,)), sems((2, pairs)), sems((2, pairs)),
             sems((count, 3, pairs)), sems((count, 3, pairs)), sems((count, group)), sems((count, group)),
             sems((4, pairs)), sems((3,)),
         ],

time: 58.2 us -> 53.8 us (0.924)
  Pallas kernels: 57.4 us -> 53 us
    pallas_call x1, Pallas kernels: 55.7 us -> 51.3 us  [body(): pl.pallas_call(functools.partial(kernel, sp, tp), in_specs=[hbm] * 7, out...]
where the time goes in v3:
time: 53.8 us; the launch traced here: 53.7 us
  Pallas kernels  53 us (99%)
  between operations  0.64 us (1%)
    pallas_call x1, Pallas kernels, body(): pl.pallas_call(functools.partial(kernel, sp, tp), in_specs=[hbm] * 7, out...  51.3 us
    pallas_call x1, Pallas kernels, body(): pl.pallas_call(drain, in_specs=[vmem] * 4, out_specs=[hbm] * 6, out_shape...  1.67 us

profile of v3, /device:TPU:0, one launch (start us, length us, event | category | flops | bytes accessed | tf_op | source)
XLA Modules:
  0.0 53.7 jit_solution(5387574256496294526)
XLA Ops:
  0.6 51.3 %attend.1 = (bf16[640,768]{1,0:T(8,128)(2,1)S(1)}, bf16[640,768]{1,0:T(8,128)(2,1)S(1)}, bf16[640,768]{1,0:T(8,128)(2,1)S(1)}, f32[7,8,128]{2,1,0:T(8,128)S(1)}) custom-call(bf16[640,768]{1,0:T(8,128)(2,1)} %q_hbm.1, bf16[640,768]{1,0:T(8,128)(2,1)} %k_hbm.1, bf16[640,768]{1,0:T(8,128)(2,1)} %v_hbm.1, bf16[640,768]{1,0:T(8,128)(2,1)} %g_hbm.1, ...), custom_call_target="tpu_custom_call" | custom-call | tf_op jit(solution)/shard_map/attend/pallas_call | solution.py:613
  52.0 1.7 %drain.1 = (bf16[640,768]{1,0:T(8,128)(2,1)}, bf16[640,768]{1,0:T(8,128)(2,1)}, bf16[640,768]{1,0:T(8,128)(2,1)}, f32[12,320]{1,0:T(8,128)}, f32[64]{0:T(128)}, /*index=5*/f32[64]{0:T(128)}) custom-call(bf16[640,768]{1,0:T(8,128)(2,1)S(1)} %get-tuple-element.10.qg_ref, bf16[640,768]{1,0:T(8,128)(2,1)S(1)} %get-tuple-element.11.kg_ref, ...), custom_call_target="tpu_custom_call" | custom-call | tf_op jit(solution)/shard_map/drain/pallas_call | solution.py:647

commit v4 on v3

--- a/solution.py
+++ b/solution.py
@@ -15,8 +15,9 @@
 BLK = 2 * SEG
 BAND = REACH + BLK
 NEG = -1e30
-LAG = 2
-AHEAD = 2
+SLOTS = 4
+BIASES = 3
+PLANE = 4
 PART = 32
 EARLY = 2
 F32 = jnp.float32
@@ -118,21 +119,23 @@
 def kernel(
     sp, tp, q_hbm, k_hbm, v_hbm, g_hbm, qgain_hbm, kgain_hbm, table_hbm,
     qg_ref, kg_ref, vg_ref, out_ref,
-    q_ref, k_ref, v_ref, g_ref,
-    k_s, kt_s, qs_s, gs_s, khat_s, kscale_s, qhat_s, qscale_s, nhat_s, dq_s,
-    bias_s, acc_s, clip_s, e_s, dw_s, peak_s, factor_s, delta_s, ds_s, w_s, gq_s, gk_s,
+    v_ref, k_s, kt_s, qs_s, gs_s, kscale_s, qscale_s, nhat_s, dq_s,
+    bias_s, acc_s, clip_s, e_s, dw_s, later_e_s, later_dw_s, peak_s, factor_s, delta_s, ds_s, w_s, gq_s, gk_s,
     nq_s, ng_s, cq_s, bq_s, mid_s, own_s, next_s, before_s, after_s,
     bsum_s, bgot_s, gsum_s, ggot_s, gfirst_s,
     qgain_s, kgain_s, raw_s, wide_s, table_s, gains_s,
     rows_send, rows_recv, back_send, back_recv, part_send, part_recv,
     bias_send, bias_recv, gain_send, gain_recv, load_sem, small_sem,
 ):
-    tokens = q_ref.shape[0]
+    q_ref, k_ref, g_ref = qg_ref, kg_ref, vg_ref
+    tokens = v_ref.shape[0]
     blocks = tokens // BLK
     cross = REACH // BLK
     pairs = nq_s.shape[0]
-    tiles = {}
+    tiles, own_tiles = {}, 0
     for qb in range(blocks + cross):
+        if qb == blocks:
+            own_tiles = len(tiles)
         for kb in range(max(qb - cross, 0), min(qb + 1, blocks)):
             tiles[qb, kb] = len(tiles)
     me = lax.axis_index("sp")
@@ -144,6 +147,8 @@
     combos = [(k, t) for k in range(rounds[0][1]) for t in range(tp) if k or t]
     nearby = [{"sp": peer(me, 1, rounds[0][1], k), "tp": lax.rem(me_tp + t, tp)} for k, t in combos]
     first, last = me == 0, me == sp - 1
+    far = lax.rem(me, PLANE) == 0
+    near_by = jnp.logical_not(far)
     has_left, has_right = jnp.logical_not(first), jnp.logical_not(last)
 
     def tile(j):
@@ -151,6 +156,11 @@
 
     def wide_tile(j):
         return slice(j * 2 * BLK, (j + 1) * 2 * BLK)
+
+    def held_at(p, place):
+        if place < own_tiles:
+            return e_s, dw_s, lax.rem(p, SLOTS), place
+        return later_e_s, later_dw_s, lax.rem(p, SLOTS - 1), place - own_tiles
 
     def lanes_of(p):
         return pl.ds(pl.multiple_of(p * BLK, BLK), BLK)
@@ -176,94 +186,6 @@
     greeted = [{"sp": right}, {"sp": left}] + nearby + [device for group in peers for device in group]
     for device in greeted:
         pl.semaphore_signal(barrier, inc=1, device_id=device, device_id_type=pl.DeviceIdType.MESH)
-    pl.semaphore_wait(barrier, len(greeted))
-
-    def remote(src, dst, send, recv, device):
-        return pltpu.make_async_remote_copy(
-            src_ref=src, dst_ref=dst, send_sem=send, recv_sem=recv,
-            device_id=device, device_id_type=pl.DeviceIdType.MESH,
-        )
-
-    def row_copies(p):
-        rows = slice(0, REACH)
-        return (
-            remote(q_hbm.at[rows, lanes_of(p)], nq_s.at[p], rows_send.at[0, p], rows_recv.at[0, p], {"sp": left}),
-            remote(g_hbm.at[rows, lanes_of(p)], ng_s.at[p], rows_send.at[1, p], rows_recv.at[1, p], {"sp": left}),
-        )
-
-    def back_copy(p):
-        return remote(cq_s.at[p], bq_s.at[p], back_send.at[p], back_recv.at[p], {"sp": right})
-
-    def own_copy(p):
-        return remote(own_s.at[p], after_s.at[p], part_send.at[0, p], part_recv.at[0, p], {"sp": left})
-
-    def next_copy(p):
-        return remote(next_s.at[p], before_s.at[p], part_send.at[1, p], part_recv.at[1, p], {"sp": right})
-
-    @pl.when(has_left)
-    def _():
-        for p in range(min(AHEAD, pairs)):
-            for copy in row_copies(p):
-                copy.start()
-
-    @pl.when(first)
-    def _():
-        bq_s[...] = jnp.zeros_like(bq_s)
-        before_s[...] = jnp.zeros_like(before_s)
-        for p in range(pairs):
-            before_s[p, 0:cross, :] = jnp.full((cross, 2 * BLK), NEG, F32)
-
-    @pl.when(last)
-    def _():
-        nq_s[...] = jnp.zeros_like(nq_s)
-        ng_s[...] = jnp.zeros_like(ng_s)
-        after_s[...] = jnp.zeros_like(after_s)
-        for p in range(pairs):
-            after_s[p, 0:cross, :] = jnp.full((cross, 2 * BLK), -NEG, F32)
-            after_s[p, cross : 2 * cross, :] = jnp.ones((cross, 2 * BLK), F32)
-
-    def bias_copies(p):
-        return [
-            remote(bsum_s.at[0, p], bgot_s.at[0, k, p], bias_send.at[0, k, p], bias_recv.at[0, k, p], device)
-            for k, device in enumerate(peers[0])
-        ]
-
-    def late_copies(r):
-        return [
-            remote(bsum_s.at[r], bgot_s.at[r, k], bias_send.at[r, k, 0], bias_recv.at[r, k, 0], device)
-            for k, device in enumerate(peers[r])
-        ]
-
-    def bias_add(r):
-        for copy in [copy for p in range(pairs) for copy in bias_copies(p)] if r == 0 else late_copies(r):
-            copy.wait_recv()
-        bsum_s[r + 1] = ring_sum([bsum_s[r]] + [bgot_s[r, k] for k in range(len(peers[r]))])
-
-    def gain_copies(r):
-        if r == 0:
-            return [
-                remote(gsum_s.at[0], gfirst_s.at[n], gain_send.at[0, n], gain_recv.at[0, n], device)
-                for n, device in enumerate(nearby)
-            ]
-        return [
-            remote(gsum_s.at[r], ggot_s.at[r, k], gain_send.at[r, k], gain_recv.at[r, k], device)
-            for k, device in enumerate(peers[r])
-        ]
-
-    def gain_start(r):
-        for copy in gain_copies(r):
-            copy.start()
-
-    def gain_add(r):
-        for copy in gain_copies(r):
-            copy.wait_recv()
-        if r == 0:
-            parts = {combo: gfirst_s[n] for n, combo in enumerate(combos)}
-            parts[0, 0] = gsum_s[0]
-            gsum_s[1] = ring_sum([ring_sum([parts[k, t] for t in range(tp)]) for k in range(rounds[0][1])])
-        else:
-            gsum_s[r + 1] = ring_sum([gsum_s[r]] + [ggot_s[r, k] for k in range(len(peers[r]))])
-
     ones = half_ones()
     for copy in smalls:
         copy.wait()
@@ -279,6 +201,111 @@
     place = lax.broadcasted_iota(jnp.int32, wide.shape, 1)
     moved = pltpu.roll(wide, 193, 1)
     table_s[...] = jnp.where(place <= 128, wide[:, span - 1 : span], jnp.where(place < 193, NEG, moved))
+
+    def next_bias(p):
+        for head in range(2):
+            build_bias(table_s[pl.ds(p * 2 + head, 1), :], bias_s.at[lax.rem(p, BIASES)], head)
+
+    for p in range(min(2, pairs)):
+        next_bias(p)
+    pl.semaphore_wait(barrier, len(greeted))
+
+    def remote(src, dst, send, recv, device):
+        return pltpu.make_async_remote_copy(
+            src_ref=src, dst_ref=dst, send_sem=send, recv_sem=recv,
+            device_id=device, device_id_type=pl.DeviceIdType.MESH,
+        )
+
+    def row_copies(p):
+        rows = slice(0, REACH)
+        return (
+            remote(q_hbm.at[rows, lanes_of(p)], nq_s.at[p], rows_send.at[0, p], rows_recv.at[0, p], {"sp": left}),
+            remote(g_hbm.at[rows, lanes_of(p)], ng_s.at[p], rows_send.at[1, p], rows_recv.at[1, p], {"sp": left}),
+        )
+
+    def back_copy(p):
+        return remote(cq_s.at[p], bq_s.at[p], back_send.at[p], back_recv.at[p], {"sp": right})
+
+    def own_copy(p):
+        return remote(own_s.at[p], after_s.at[p], part_send.at[0, p], part_recv.at[0, p], {"sp": left})
+
+    def next_copy(p):
+        return remote(next_s.at[p], before_s.at[p], part_send.at[1, p], part_recv.at[1, p], {"sp": right})
+
+    @pl.when(has_left)
+    def _():
+        for copy in row_copies(0):
+            copy.start()
+
+    @pl.when(has_left)
+    def _():
+        for copy in row_copies(1):
+            copy.start()
+
+    @pl.when(first)
+    def _():
+        bq_s[...] = jnp.zeros_like(bq_s)
+        before_s[...] = jnp.zeros_like(before_s)
+        for p in range(pairs):
+            before_s[p, 0:cross, :] = jnp.full((cross, 2 * BLK), NEG, F32)
+
+    @pl.when(last)
+    def _():
+        nq_s[...] = jnp.zeros_like(nq_s)
+        ng_s[...] = jnp.zeros_like(ng_s)
+        after_s[...] = jnp.zeros_like(after_s)
+        for p in range(pairs):
+            after_s[p, 0:cross, :] = jnp.full((cross, 2 * BLK), -NEG, F32)
+            after_s[p, cross : 2 * cross, :] = jnp.ones((cross, 2 * BLK), F32)
+
+    early = pairs - 1
+
+    def bias_copies(p):
+        return [
+            remote(bsum_s.at[0, p], bgot_s.at[0, k, p], bias_send.at[0, k, p], bias_recv.at[0, k, p], device)
+            for k, device in enumerate(peers[0])
+        ]
+
+    def late_copies(r):
+        return [
+            remote(bsum_s.at[r], bgot_s.at[r, k], bias_send.at[r, k, 0], bias_recv.at[r, k, 0], device)
+            for k, device in enumerate(peers[r])
+        ]
+
+    def bias_add(r):
+        for copy in [copy for p in range(early) for copy in bias_copies(p)] if r == 0 else late_copies(r):
+            copy.wait_recv()
+        bsum_s[r + 1] = ring_sum([bsum_s[r]] + [bgot_s[r, k] for k in range(len(peers[r]))])
+        if r + 1 < count:
+            for copy in late_copies(r + 1):
+                copy.start()
+
+    def gain_copies(r):
+        if r == 0:
+            return [
+                remote(gsum_s.at[0], gfirst_s.at[n], gain_send.at[0, n], gain_recv.at[0, n], device)
+                for n, device in enumerate(nearby)
+            ]
+        return [
+            remote(gsum_s.at[r], ggot_s.at[r, k], gain_send.at[r, k], gain_recv.at[r, k], device)
+            for k, device in enumerate(peers[r])
+        ]
+
+    def gain_start(r):
+        for copy in gain_copies(r):
+            copy.start()
+
+    def gain_add(r):
+        for copy in gain_copies(r):
+            copy.wait_recv()
+        if r == 0:
+            parts = {combo: gfirst_s[n] for n, combo in enumerate(combos)}
+            parts[0, 0] = gsum_s[0]
+            gsum_s[1, 0] = ring_sum([parts[k, 0][0] for k in range(rounds[0][1])])
+            gsum_s[1, 1] = ring_sum([ring_sum([parts[k, t][1] for t in range(tp)]) for k in range(rounds[0][1])])
+        else:
+            gsum_s[r + 1] = ring_sum([gsum_s[r]] + [ggot_s[r, k] for k in range(len(peers[r]))])
+
     gq_s[...] = jnp.zeros_like(gq_s)
     gk_s[...] = jnp.zeros_like(gk_s)
 
@@ -293,13 +320,14 @@
         for kb in range(max(qb - cross, 0), min(qb + 1, blocks)):
             place = tiles[qb, kb]
             j = kb - qb + cross
-            s = dot(k_s[slot, tile(kb), :], qs_s[slot, wide_tile(qb), :], ((1,), (1,))) + bias_s[tile(j), :]
+            s = dot(k_s[slot, tile(kb), :], qs_s[slot, wide_tile(qb), :], ((1,), (1,))) + bias_s[lax.rem(p, BIASES), tile(j), :]
             s = grouped(s)
             peak = jnp.max(s, axis=0)
             e = jnp.exp(s - peak[None])
             dw = dot(v_ref[tile(kb), lanes_of(p)], gs_s[slot, wide_tile(qb), :], ((1,), (1,)))
-            e_s[slot, place] = e.reshape(BLK, 2 * BLK)
-            dw_s[slot, place] = dw
+            e_ref, dw_ref, at, spot = held_at(p, place)
+            e_ref[at, spot] = e.reshape(BLK, 2 * BLK)
+            dw_ref[at, spot] = dw
             peak_s[slot, place] = peak
             peaks.append(peak)
             sums.append(jnp.sum(e, axis=0))
@@ -321,45 +349,38 @@
                 at = n * cross + qb - blocks
                 next_s[p, at : at + 1, :] = row
 
-    def forward(p):
-        slot = lax.rem(p, 2)
+    def inner(p):
+        slot = lax.rem(p, SLOTS)
         for copy in loads(p):
             copy.wait()
 
         def prepare(b):
             hat, scale = normed(k_ref[tile(b), lanes_of(p)], ones)
-            khat_s[slot, tile(b), :] = hat
             kscale_s[slot, tile(b), :] = scale
             unit = hat * gain_k
             k_s[slot, tile(b), :] = unit.astype(BF16)
-            kt_s[lax.rem(p, 3), :, tile(b)] = unit.T.astype(BF16)
-            hat, scale = query_tile(slot, b, q_ref[tile(b), lanes_of(p)], g_ref[tile(b), lanes_of(p)])
-            qhat_s[p, tile(b), :] = hat
+            kt_s[lax.rem(p, SLOTS + 1), :, tile(b)] = unit.T.astype(BF16)
+            _, scale = query_tile(slot, b, q_ref[tile(b), lanes_of(p)], g_ref[tile(b), lanes_of(p)])
             qscale_s[p, tile(b), :] = scale
 
-        past = jnp.maximum(p - 2, 0)
         for b in range(EARLY):
             prepare(b)
         for b in range(blocks):
             if b + EARLY < blocks:
                 prepare(b + EARLY)
-            rest_query(past, b, p >= 2)
             scores(p, slot, b)
-        rest_bias(past)
-
-        @pl.when(p >= 2)
-        def _():
-            for copy in bias_copies(past):
+
+        @pl.when(has_left)
+        def _():
+            own_copy(p).start()
+
+        @pl.when(has_left & near_by & (p == 0))
+        def _():
+            for copy in row_copies(2):
                 copy.start()
 
-        @pl.when(has_left)
-        def _():
-            own_copy(p).start()
-
-        @pl.when(has_left & (p + AHEAD < pairs))
-        def _():
-            for copy in row_copies(p + AHEAD):
-                copy.start()
+    def outer(p):
+        slot = lax.rem(p, SLOTS)
 
         @pl.when(has_right)
         def _():
@@ -369,16 +390,18 @@
         for b in range(cross):
             hat, _ = query_tile(slot, blocks + b, nq_s[p, tile(b), :], ng_s[p, tile(b), :])
             nhat_s[slot, tile(b), :] = hat
+        past = jnp.maximum(p - 3, 0)
         for b in range(cross):
+            rest_query(past, b, p >= 3)
             scores(p, slot, blocks + b)
+        for b in range(cross, blocks):
+            rest_query(past, b, p >= 3)
+        bsum_s[0, past] = rest_bias(past)
+        next_bias(jnp.minimum(p + 2, pairs - 1))
 
         @pl.when(has_right)
         def _():
             next_copy(p).start()
-
-    def next_bias(p):
-        for head in range(2):
-            build_bias(table_s[pl.ds(p * 2 + head, 1), :], bias_s, head)
 
     def settle(mine, other):
         here, there = mine[:cross], other[:cross]
@@ -390,7 +413,7 @@
         return peak, inverse, delta * inverse
 
     def backward(p):
-        slot = lax.rem(p, 2)
+        slot = lax.rem(p, SLOTS)
 
         @pl.when(has_left)
         def _():
@@ -399,6 +422,11 @@
         @pl.when(has_right)
         def _():
             own_copy(p).wait_recv()
+
+        @pl.when(has_left & (p + 3 < pairs) & (p <= 1) & far)
+        def _():
+            for copy in row_copies(p + 3):
+                copy.start()
 
         own = settle(own_s[p], before_s[p])
         later = settle(next_s[p], after_s[p])
@@ -417,10 +445,11 @@
         for kb in reversed(range(blocks)):
             for qb in range(kb, kb + cross + 1):
                 place, j = tiles[qb, kb], kb - qb + cross
+                e_ref, dw_ref, held, spot = held_at(p, place)
                 for part in range(BLK // PART):
                     rows = slice(part * PART, (part + 1) * PART)
-                    w = grouped(e_s[slot, place, rows, :]) * factor_s[place][None]
-                    ds = w * (grouped(dw_s[slot, place, rows, :]) - delta_s[qb][None])
+                    w = grouped(e_ref[held, spot, rows, :]) * factor_s[place][None]
+                    ds = w * (grouped(dw_ref[held, spot, rows, :]) - delta_s[qb][None])
                     if j < 2:
                         clipped = clipped + jnp.sum(ds, axis=0)
                     ds, w = ds.reshape(PART, 2 * BLK), w.reshape(PART, 2 * BLK)
@@ -430,14 +459,14 @@
                     at = slice(kb * BLK + part * PART, kb * BLK + (part + 1) * PART)
                     ds_s[at, wide_tile(qb)] = ds.astype(BF16)
                     w_s[at, wide_tile(qb)] = w.astype(BF16)
-            inner = slice(kb * 2 * BLK, blocks * 2 * BLK)
-            outer = slice(blocks * 2 * BLK, (kb + cross + 1) * 2 * BLK)
-            dk = dot(ds_s[tile(kb), inner], qs_s[slot, inner, :], ((1,), (0,)))
-            dv = dot(w_s[tile(kb), inner], gs_s[slot, inner, :], ((1,), (0,)))
+            near = slice(kb * 2 * BLK, blocks * 2 * BLK)
+            away = slice(blocks * 2 * BLK, (kb + cross + 1) * 2 * BLK)
+            dk = dot(ds_s[tile(kb), near], qs_s[slot, near, :], ((1,), (0,)))
+            dv = dot(w_s[tile(kb), near], gs_s[slot, near, :], ((1,), (0,)))
             if kb + cross >= blocks:
-                dk = dk + dot(ds_s[tile(kb), outer], qs_s[slot, outer, :], ((1,), (0,))).astype(BF16).astype(F32)
-                dv = dv + dot(w_s[tile(kb), outer], gs_s[slot, outer, :], ((1,), (0,))).astype(BF16).astype(F32)
-            hat = khat_s[slot, tile(kb), :]
+                dk = dk + dot(ds_s[tile(kb), away], qs_s[slot, away, :], ((1,), (0,))).astype(BF16).astype(F32)
+                dv = dv + dot(w_s[tile(kb), away], gs_s[slot, away, :], ((1,), (0,))).astype(BF16).astype(F32)
+            hat = k_ref[tile(kb), lanes_of(p)].astype(F32) * kscale_s[slot, tile(kb), :]
             gain_sum = gain_sum + jnp.sum(dk * hat, axis=0, keepdims=True)
             kg_ref[tile(kb), lanes_of(p)] = norm_grad(dk, gain_k, hat, kscale_s[slot, tile(kb), :], ones).astype(BF16)
             vg_ref[tile(kb), lanes_of(p)] = dv.astype(BF16)
@@ -445,7 +474,6 @@
                 query_side(p, slot, kb + cross)
         gk_s[...] += gain_sum
         clip_s[...] = clipped
-        next_bias(jnp.minimum(p + 2, pairs - 1))
 
         @pl.when(has_right)
         def _():
@@ -453,7 +481,7 @@
 
     def turned(p, qb):
         keys = slice(max(qb - cross, 0) * BLK, min(qb + 1, blocks) * BLK)
-        dqt = dot(kt_s[lax.rem(p, 3), :, keys], ds_s[keys, wide_tile(qb)], ((1,), (0,)))
+        dqt = dot(kt_s[lax.rem(p, SLOTS + 1), :, keys], ds_s[keys, wide_tile(qb)], ((1,), (0,)))
         dqt = jnp.concatenate([dqt[:64, :BLK], dqt[64:, BLK:]], axis=0)
         return dqt.T * 0.125
 
@@ -465,7 +493,8 @@
     def rest_query(p, qb, live):
         dq = turned(p, qb)
         dq_s[p, tile(qb), :] = dq
-        part = jnp.sum(dq * qhat_s[p, tile(qb), :], axis=0, keepdims=True)
+        hat = q_ref[tile(qb), lanes_of(p)].astype(F32) * qscale_s[p, tile(qb), :]
+        part = jnp.sum(dq * hat, axis=0, keepdims=True)
         gq_s[...] += jnp.where(live, part, 0.0)
 
     def rest_bias(p):
@@ -476,14 +505,7 @@
             far = jnp.sum(clipped[:, head * BLK : (head + 1) * BLK], axis=1, keepdims=True)
             row = fold_bias(acc_s, head) + jnp.where(lane == 0, far, 0.0)
             rows += [row[:, b * BLK : (b + 1) * BLK] for b in range(4)]
-        bsum_s[0, p] = jnp.concatenate(rows, axis=0)
-
-    def rest(p):
-        for qb in range(blocks):
-            rest_query(p, qb, True)
-        rest_bias(p)
-        for copy in bias_copies(p):
-            copy.start()
+        return jnp.concatenate(rows, axis=0)
 
     def finish(p, _):
         @pl.when(has_left)
@@ -494,7 +516,9 @@
             dq = dq_s[p, tile(b), :]
             if b < cross:
                 dq = dq + bq_s[p, tile(b), :].astype(F32)
-            grad = norm_grad(dq, gain_q, qhat_s[p, tile(b), :], qscale_s[p, tile(b), :], ones)
+            scale = qscale_s[p, tile(b), :]
+            hat = q_ref[tile(b), lanes_of(p)].astype(F32) * scale
+            grad = norm_grad(dq, gain_q, hat, scale, ones)
             qg_ref[tile(b), lanes_of(p)] = grad.astype(BF16)
 
         @pl.when(has_left)
@@ -507,53 +531,73 @@
             for copy in (back_copy(p), next_copy(p)):
                 copy.wait_send()
 
-        for copy in bias_copies(p):
-            copy.wait_send()
         return 0
 
     def step(t, _):
         @pl.when(t < pairs)
         def _():
-            forward(t)
-
-        @pl.when(t == pairs)
-        def _():
-            rest(pairs - 2)
-
-        @pl.when(t == 0)
-        def _():
-            next_bias(min(1, pairs - 1))
-
-        @pl.when(t >= 1)
-        def _():
-            backward(t - 1)
-
-        @pl.when(t >= 1 + LAG)
-        def _():
-            finish(t - 1 - LAG, 0)
+            inner(t)
+
+        @pl.when((t >= 1) & (t <= pairs))
+        def _():
+            outer(t - 1)
+
+        @pl.when(has_left & (t < pairs) & (t == 2) & far)
+        def _():
+            for copy in row_copies(t):
+                copy.start()
+
+        @pl.when(has_left & (t + 2 < pairs) & (t >= 1) & near_by)
+        def _():
+            for copy in row_copies(t + 2):
+                copy.start()
+
+        @pl.when(t > pairs)
+        def _():
+            for qb in range(blocks):
+                rest_query(t - 4, qb, True)
+            bsum_s[0, t - 4] = rest_bias(t - 4)
+
+        @pl.when(t >= 4)
+        def _():
+            for copy in bias_copies(t - 4):
+                copy.start()
+
+        @pl.when(t >= 3)
+        def _():
+            backward(t - 3)
+
+        @pl.when(has_left & (t >= 4) & (t + 1 < pairs) & far)
+        def _():
+            for copy in row_copies(t + 1):
+                copy.start()
 
         return 0
 
-    next_bias(0)
-    lax.fori_loop(0, pairs + 1, step, 0)
-    rest(pairs - 1)
-    gsum_s[0] = jnp.zeros(gsum_s.shape[1:], F32)
-    gsum_s[0, 0:1, :] = gq_s[...]
-    gsum_s[0, 1:2, :] = gk_s[...]
+    lax.fori_loop(0, pairs + 3, step, 0)
+    for qb in range(blocks):
+        rest_query(pairs - 1, qb, True)
+    gsum_s[0, 0] = rest_bias(pairs - 1)
+    gsum_s[0, 1] = jnp.zeros(gsum_s.shape[2:], F32)
+    gsum_s[0, 1, 0:1, :] = gq_s[...]
+    gsum_s[0, 1, 1:2, :] = gk_s[...]
     gain_start(0)
     for r in range(count):
         bias_add(r)
-        if r + 1 < count:
-            for copy in late_copies(r + 1):
-                copy.start()
+        if r == 0:
+            lax.fori_loop(0, pairs // 2, finish, 0)
         gain_add(r)
         if r + 1 < count:
             gain_start(r + 1)
-    lax.fori_loop(max(pairs - LAG, 0), pairs, finish, 0)
-    for p in range(pairs):
+        if r == 0:
+            lax.fori_loop(pairs // 2, pairs, finish, 0)
+    for p in range(early):
         out_ref[p] = bsum_s[count, p]
-    out_ref[pairs] = gsum_s[count]
-
+    out_ref[early] = gsum_s[count, 0]
+    out_ref[pairs] = gsum_s[count, 1]
+    for p in range(early):
+        for copy in bias_copies(p):
+            copy.wait_send()
     for r in range(count):
         if r > 0:
             for copy in late_copies(r):
@@ -600,7 +644,9 @@
     count = len(rounds_of(sp))
     group = 4 * tp
     ext = tokens + REACH
-    held = (REACH // BLK + 1) * (tokens // BLK)
+    reach, blocks = REACH // BLK, tokens // BLK
+    held = (reach + 1) * blocks
+    own = sum(min(qb, reach) + 1 for qb in range(blocks))
     padded = (heads + 7) // 8 * 8
     vmem, hbm = pl.BlockSpec(memory_space=pltpu.VMEM), pl.BlockSpec(memory_space=pltpu.HBM)
     shape = jax.ShapeDtypeStruct
@@ -615,33 +661,32 @@
         in_specs=[hbm] * 7,
         out_specs=[vmem] * 4,
         out_shape=[grads, grads, grads, shape((pairs + 1, 8, BLK), F32)],
-        scratch_shapes=[pltpu.VMEM((tokens, heads * 64), BF16)] * 4
+        scratch_shapes=[pltpu.VMEM((tokens, heads * 64), BF16)]
         + [
-            pltpu.VMEM((2, tokens, BLK), BF16), pltpu.VMEM((3, BLK, tokens), BF16),
-            pltpu.VMEM((2, ext * 2, BLK), BF16), pltpu.VMEM((2, ext * 2, BLK), BF16),
-            pltpu.VMEM((2, tokens, BLK), F32), pltpu.VMEM((2, tokens, BLK), F32),
-            pltpu.VMEM((pairs, tokens, BLK), F32), pltpu.VMEM((pairs, tokens, BLK), F32),
-            pltpu.VMEM((2, REACH, BLK), F32), pltpu.VMEM((pairs, tokens, BLK), F32),
-            pltpu.VMEM((BAND, 2 * BLK), F32), pltpu.VMEM((3 * BLK, 2 * BLK), F32), pltpu.VMEM((8, 2 * BLK), F32),
-            pltpu.VMEM((2, held, BLK, 2 * BLK), F32), pltpu.VMEM((2, held, BLK, 2 * BLK), F32),
-            pltpu.VMEM((2, held, 8, 2 * BLK), F32), pltpu.VMEM((held, 8, 2 * BLK), F32),
+            pltpu.VMEM((SLOTS, tokens, BLK), BF16), pltpu.VMEM((SLOTS + 1, BLK, tokens), BF16),
+            pltpu.VMEM((SLOTS, ext * 2, BLK), BF16), pltpu.VMEM((SLOTS, ext * 2, BLK), BF16),
+            pltpu.VMEM((SLOTS, tokens, BLK), F32), pltpu.VMEM((pairs, tokens, BLK), F32),
+            pltpu.VMEM((SLOTS, REACH, BLK), F32), pltpu.VMEM((pairs, tokens, BLK), F32),
+            pltpu.VMEM((BIASES, BAND, 2 * BLK), F32), pltpu.VMEM((3 * BLK, 2 * BLK), F32), pltpu.VMEM((8, 2 * BLK), F32),
+            *[pltpu.VMEM((SLOTS, own, BLK, 2 * BLK), F32)] * 2, *[pltpu.VMEM((SLOTS - 1, held - own, BLK, 2 * BLK), F32)] * 2,
+            pltpu.VMEM((SLOTS, held, 8, 2 * BLK), F32), pltpu.VMEM((held, 8, 2 * BLK), F32),
             pltpu.VMEM((ext // BLK, 8, 2 * BLK), F32),
             pltpu.VMEM((tokens, ext * 2), BF16), pltpu.VMEM((tokens, ext * 2), BF16),
             pltpu.VMEM((1, BLK), F32), pltpu.VMEM((1, BLK), F32),
         ]
         + [pltpu.VMEM((pairs, REACH, BLK), BF16)] * 4
-        + [pltpu.VMEM((2, 8, 2 * BLK), F32)]
+        + [pltpu.VMEM((SLOTS, 8, 2 * BLK), F32)]
         + [pltpu.VMEM((pairs, 16, 2 * BLK), F32)] * 4
         + [
-            pltpu.VMEM((count + 1, pairs, 8, BLK), F32), pltpu.VMEM((count, 3, pairs, 8, BLK), F32),
-            pltpu.VMEM((count + 1, 8, BLK), F32), pltpu.VMEM((count, 3, 8, BLK), F32), pltpu.VMEM((group, 8, BLK), F32),
+            pltpu.VMEM((count + 1, pairs - 1, 8, BLK), F32), pltpu.VMEM((count, 3, pairs - 1, 8, BLK), F32),
+            pltpu.VMEM((count + 1, 2, 8, BLK), F32), pltpu.VMEM((count, 3, 2, 8, BLK), F32), pltpu.VMEM((group, 2, 8, BLK), F32),
             pltpu.VMEM((1, 64), BF16), pltpu.VMEM((1, 64), BF16), pltpu.VMEM(position_bias.shape, BF16),
             pltpu.VMEM((padded, 512), F32), pltpu.VMEM((padded, 512), F32), pltpu.VMEM((8, BLK), F32),
             sems((2, pairs)), sems((2, pairs)), sems((pairs,)), sems((pairs,)), sems((2, pairs)), sems((2, pairs)),
             sems((count, 3, pairs)), sems((count, 3, pairs)), sems((count, group)), sems((count, group)),
             sems((4, pairs)), sems((3,)),
         ],
-        compiler_params=pltpu.CompilerParams(collective_id=0, has_side_effects=True, vmem_limit_bytes=48 << 20),
+        compiler_params=pltpu.CompilerParams(collective_id=0, has_side_effects=True, vmem_limit_bytes=50 << 20),
         name="attend",
     )(*[pltpu.with_memory_space_constraint(x, pltpu.HBM) for x in operands])
     return pl.pallas_call(

time: 53.8 us -> 49.9 us (0.928)
  Pallas kernels: 53 us -> 49.1 us
    pallas_call x1, Pallas kernels: 51.3 us -> 47.5 us  [body(): pl.pallas_call(functools.partial(kernel, sp, tp), in_specs=[hbm] * 7, out...]
where the time goes in v4:
time: 49.9 us; the launch traced here: 49.8 us
  Pallas kernels  49.1 us (98%)
  between operations  0.64 us (1%)
    pallas_call x1, Pallas kernels, body(): pl.pallas_call(functools.partial(kernel, sp, tp), in_specs=[hbm] * 7, out...  47.5 us
    pallas_call x1, Pallas kernels, body(): pl.pallas_call(drain, in_specs=[vmem] * 4, out_specs=[hbm] * 6, out_shape...  1.67 us

profile of v4, /device:TPU:0, one launch (start us, length us, event | category | flops | bytes accessed | tf_op | source)
XLA Modules:
  0.0 49.8 jit_solution(8013923889586396510)
XLA Ops:
  0.6 47.5 %attend.1 = (bf16[640,768]{1,0:T(8,128)(2,1)S(1)}, bf16[640,768]{1,0:T(8,128)(2,1)S(1)}, bf16[640,768]{1,0:T(8,128)(2,1)S(1)}, f32[7,8,128]{2,1,0:T(8,128)S(1)}) custom-call(bf16[640,768]{1,0:T(8,128)(2,1)} %q_hbm.1, bf16[640,768]{1,0:T(8,128)(2,1)} %k_hbm.1, bf16[640,768]{1,0:T(8,128)(2,1)} %v_hbm.1, bf16[640,768]{1,0:T(8,128)(2,1)} %g_hbm.1, ...), custom_call_target="tpu_custom_call" | custom-call | tf_op jit(solution)/shard_map/attend/pallas_call | solution.py:659
  48.1 1.7 %drain.1 = (bf16[640,768]{1,0:T(8,128)(2,1)}, bf16[640,768]{1,0:T(8,128)(2,1)}, bf16[640,768]{1,0:T(8,128)(2,1)}, f32[12,320]{1,0:T(8,128)}, f32[64]{0:T(128)}, /*index=5*/f32[64]{0:T(128)}) custom-call(bf16[640,768]{1,0:T(8,128)(2,1)S(1)} %get-tuple-element.10.qg_ref, bf16[640,768]{1,0:T(8,128)(2,1)S(1)} %get-tuple-element.11.kg_ref, ...), custom_call_target="tpu_custom_call" | custom-call | tf_op jit(solution)/shard_map/drain/pallas_call | solution.py:692

commit v5 on v4

--- a/solution.py
+++ b/solution.py
@@ -18,7 +18,7 @@
 SLOTS = 4
 BIASES = 3
 PLANE = 4
-PART = 32
+PART = 16
 EARLY = 2
 F32 = jnp.float32
 BF16 = jnp.bfloat16
@@ -186,28 +186,10 @@
     greeted = [{"sp": right}, {"sp": left}] + nearby + [device for group in peers for device in group]
     for device in greeted:
         pl.semaphore_signal(barrier, inc=1, device_id=device, device_id_type=pl.DeviceIdType.MESH)
-    ones = half_ones()
-    for copy in smalls:
-        copy.wait()
-    for half in range(2):
-        gains_s[0:1, half * 64 : half * 64 + 64] = qgain_s[...].astype(F32)
-        gains_s[1:2, half * 64 : half * 64 + 64] = kgain_s[...].astype(F32)
-    gain_q = gains_s[0:1, :]
-    gain_k = gains_s[1:2, :]
-    heads, span = raw_s.shape
-    wide_s[...] = jnp.zeros_like(wide_s)
-    wide_s[0:heads, 0:span] = raw_s[...].astype(F32)
-    wide = wide_s[...]
-    place = lax.broadcasted_iota(jnp.int32, wide.shape, 1)
-    moved = pltpu.roll(wide, 193, 1)
-    table_s[...] = jnp.where(place <= 128, wide[:, span - 1 : span], jnp.where(place < 193, NEG, moved))
-
     def next_bias(p):
         for head in range(2):
             build_bias(table_s[pl.ds(p * 2 + head, 1), :], bias_s.at[lax.rem(p, BIASES)], head)
 
-    for p in range(min(2, pairs)):
-        next_bias(p)
     pl.semaphore_wait(barrier, len(greeted))
 
     def remote(src, dst, send, recv, device):
@@ -538,14 +520,14 @@
         def _():
             inner(t)
 
-        @pl.when((t >= 1) & (t <= pairs))
-        def _():
-            outer(t - 1)
-
         @pl.when(has_left & (t < pairs) & (t == 2) & far)
         def _():
             for copy in row_copies(t):
                 copy.start()
+
+        @pl.when((t >= 1) & (t <= pairs))
+        def _():
+            outer(t - 1)
 
         @pl.when(has_left & (t + 2 < pairs) & (t >= 1) & near_by)
         def _():
@@ -574,6 +556,24 @@
 
         return 0
 
+    ones = half_ones()
+    for copy in smalls:
+        copy.wait()
+    for half in range(2):
+        gains_s[0:1, half * 64 : half * 64 + 64] = qgain_s[...].astype(F32)
+        gains_s[1:2, half * 64 : half * 64 + 64] = kgain_s[...].astype(F32)
+    gain_q = gains_s[0:1, :]
+    gain_k = gains_s[1:2, :]
+    heads, span = raw_s.shape
+    wide_s[...] = jnp.zeros_like(wide_s)
+    wide_s[0:heads, 0:span] = raw_s[...].astype(F32)
+    wide = wide_s[...]
+    place = lax.broadcasted_iota(jnp.int32, wide.shape, 1)
+    moved = pltpu.roll(wide, 193, 1)
+    table_s[...] = jnp.where(place <= 128, wide[:, span - 1 : span], jnp.where(place < 193, NEG, moved))
+
+    for p in range(min(2, pairs)):
+        next_bias(p)
     lax.fori_loop(0, pairs + 3, step, 0)
     for qb in range(blocks):
         rest_query(pairs - 1, qb, True)

time: 49.9 us -> 49 us (0.982)
  Pallas kernels: 49.1 us -> 48.2 us
    pallas_call x1, Pallas kernels: 47.5 us -> 46.5 us  [body(): pl.pallas_call(functools.partial(kernel, sp, tp), in_specs=[hbm] * 7, out...]
where the time goes in v5:
time: 49 us; the launch traced here: 48.8 us
  Pallas kernels  48.2 us (98%)
  between operations  0.64 us (1%)
    pallas_call x1, Pallas kernels, body(): pl.pallas_call(functools.partial(kernel, sp, tp), in_specs=[hbm] * 7, out...  46.5 us
    pallas_call x1, Pallas kernels, body(): pl.pallas_call(drain, in_specs=[vmem] * 4, out_specs=[hbm] * 6, out_shape...  1.67 us

profile of v5, /device:TPU:0, one launch (start us, length us, event | category | flops | bytes accessed | tf_op | source)
XLA Modules:
  0.0 48.8 jit_solution(4265972332932179608)
XLA Ops:
  0.6 46.5 %attend.1 = (bf16[640,768]{1,0:T(8,128)(2,1)S(1)}, bf16[640,768]{1,0:T(8,128)(2,1)S(1)}, bf16[640,768]{1,0:T(8,128)(2,1)S(1)}, f32[7,8,128]{2,1,0:T(8,128)S(1)}) custom-call(bf16[640,768]{1,0:T(8,128)(2,1)} %q_hbm.1, bf16[640,768]{1,0:T(8,128)(2,1)} %k_hbm.1, bf16[640,768]{1,0:T(8,128)(2,1)} %v_hbm.1, bf16[640,768]{1,0:T(8,128)(2,1)} %g_hbm.1, ...), custom_call_target="tpu_custom_call" | custom-call | tf_op jit(solution)/shard_map/attend/pallas_call | solution.py:659
  47.1 1.7 %drain.1 = (bf16[640,768]{1,0:T(8,128)(2,1)}, bf16[640,768]{1,0:T(8,128)(2,1)}, bf16[640,768]{1,0:T(8,128)(2,1)}, f32[12,320]{1,0:T(8,128)}, f32[64]{0:T(128)}, /*index=5*/f32[64]{0:T(128)}) custom-call(bf16[640,768]{1,0:T(8,128)(2,1)S(1)} %get-tuple-element.10.qg_ref, bf16[640,768]{1,0:T(8,128)(2,1)S(1)} %get-tuple-element.11.kg_ref, ...), custom_call_target="tpu_custom_call" | custom-call | tf_op jit(solution)/shard_map/drain/pallas_call | solution.py:692
